TPU v7x, 32 devices: a whole 2x2x4 slice. The times are simulated.
32 devices in a mesh: rep: 2 (over core), fs: 8 (over z, y), tp: 2 (over x).
Axes of the slice: x: 2, y: 2, z: 4, core: 2. Of those that a mesh axis runs over, the one named last changes fastest.
Arguments:
- tokens: bfloat16 [8192, 2048], P(('rep', 'fs')), may hold values from -6 to 6
- recurrence_branch_weight: bfloat16 [2048, 2048], P('fs', 'tp'), may hold values from -0.125 to 0.125
- gate_branch_weight: bfloat16 [2048, 2048], P('fs', 'tp'), may hold values from -0.125 to 0.125
- convolution_kernel: bfloat16 [4, 2048], P(None, 'tp'), may hold values from -3 to 3
- recurrence_gate_blockwise: bfloat16 [8, 256, 256], P('tp'), may hold values from -0.375 to 0.375
- input_gate_blockwise: bfloat16 [8, 256, 256], P('tp'), may hold values from -0.375 to 0.375
- channel_decay_param: float32 [2048], P('tp')
- token_decay_shift: float32 [8192, 2048], P(('rep', 'fs'), 'tp'), may hold values from -1 to 0
- recurrence_output_weight: bfloat16 [2048, 2048], P('tp', 'fs'), may hold values from -0.5 to 0.5
- first_norm_gain: float32 [2048], replicated, may hold values from 0.1 to 1.9
- feedforward_gate_weight: bfloat16 [2048, 5120], P('fs', 'tp'), may hold values from -0.125 to 0.125
- feedforward_up_weight: bfloat16 [2048, 5120], P('fs', 'tp'), may hold values from -0.125 to 0.125
- feedforward_down_weight: bfloat16 [5120, 2048], P('tp', 'fs'), may hold values from -0.15625 to 0.15625
- second_norm_gain: float32 [2048], replicated, may hold values from 0.1 to 1.9
Outputs:
- layer_out: bfloat16 [8192, 2048], P(('rep', 'fs', 'tp'))
All inputs are finite; a program needn't handle non-finite values.
Results may differ from a plain program's by a relative error of at most 0.02.
Values may be sent and summed in bfloat16 or wider, within the bound.
A program may use at most 128 MiB of HBM per device.

v0:
```python
import functools

import jax
import jax.numpy as jnp
from jax import lax
from jax.experimental import pallas as pl
from jax.experimental.pallas import tpu as pltpu
from jax.sharding import PartitionSpec as P


residual_scale = 1.4142135623730951


VMEM_BYTES = 60 * 1024 * 1024


def layer_norm(values, gain):
    center = values - jnp.mean(values, axis=-1, keepdims=True)
    variance = jnp.mean(center * center, axis=-1, keepdims=True)
    return center * lax.rsqrt(variance + 1e-05) * gain


def direct_plan():
    count = lax.axis_size("fs")
    return lax.axis_size("rep") == 2 and count % 2 == 0 and count <= 8


def visit_order(outer):
    return sorted(range(1, outer), key=lambda step: min(step, outer - step))


def gather_parts(shard):
    count = lax.axis_size("fs")
    outer = count // 2
    swap = [(at, at ^ 1) for at in range(count)]
    near = {0: shard}
    for step in visit_order(outer):
        pairs = [
            (at * 2 + side, ((at - step) % outer) * 2 + side)
            for at in range(outer)
            for side in range(2)
        ]
        near[step] = lax.ppermute(shard, "fs", pairs)
    far = {}
    for step in range(outer):
        far[step] = lax.ppermute(near[step], "fs", swap)
    mine = [near[step] for step in range(outer)] + [far[step] for step in range(outer)]
    other = []
    for part in mine:
        other.append(lax.ppermute(part, "rep", [(0, 1), (1, 0)]))
    return mine, other


def part_owners():
    count = lax.axis_size("fs")
    outer = count // 2
    me = lax.axis_index("fs")
    at, side = me // 2, me % 2
    return [
        ((at + step) % outer) * 2 + (side if flip == 0 else 1 - side)
        for flip in range(2)
        for step in range(outer)
    ]


def gather_two(first, second, axis):
    if direct_plan():
        core = lax.axis_index("rep")
        mine, other = gather_parts(jnp.where(core == 0, first, second))
        return mine, other, part_owners(), core
    return (
        [lax.all_gather(first, "fs", axis=axis, tiled=True)],
        [lax.all_gather(second, "fs", axis=axis, tiled=True)],
        [jnp.int32(0)],
        jnp.int32(0),
    )


def gather_halves(weight):
    half = weight.shape[0] // 2
    return gather_two(weight[:half], weight[half:], 1)


def scalars(owners, swapped):
    return jnp.stack([jnp.asarray(v, jnp.int32) for v in [swapped, *owners]])


def split_product(meta, left_ref, part_refs):
    total = None
    for at, part in enumerate(part_refs):
        depth = part.shape[0]
        columns = pl.ds(pl.multiple_of(meta[1 + at] * depth, depth), depth)
        term = jnp.dot(left_ref[:, columns], part[...], preferred_element_type=jnp.float32)
        total = term if total is None else total + term
    return total


def shifted(values, step, fill):
    rows = lax.broadcasted_iota(jnp.int32, values.shape, 0)
    return jnp.where(rows < step, fill, pltpu.roll(values, step, 0))


def sigmoid(values):
    return 1.0 / (1.0 + jnp.exp(-values))


def recurrence_kernel(count, meta, x_ref, taps_ref, rate_ref, inlet_ref, plus_ref, shift_ref, *refs):
    mine, other, out_ref = refs[:count], refs[count : 2 * count], refs[-1]
    first = split_product(meta, x_ref, mine)
    second = split_product(meta, x_ref, other)
    swapped = meta[0] == 1
    value_in = jnp.where(swapped, second, first).astype(jnp.bfloat16).astype(jnp.float32)
    gate_in = jnp.where(swapped, first, second).astype(jnp.bfloat16).astype(jnp.float32)
    taps = taps_ref[...].astype(jnp.float32)
    depth = taps.shape[0]
    conv = None
    for tap in range(depth):
        lag = depth - 1 - tap
        moved = value_in if lag == 0 else shifted(value_in, lag, 0.0)
        term = moved * taps[tap : tap + 1, :]
        conv = term if conv is None else conv + term
    conv = conv.astype(jnp.bfloat16)
    rate = sigmoid(jnp.dot(conv, rate_ref[0], preferred_element_type=jnp.float32))
    inlet = sigmoid(jnp.dot(conv, inlet_ref[0], preferred_element_type=jnp.float32))
    log_decay = -8.0 * rate * plus_ref[...] + shift_ref[...]
    decay = jnp.exp(log_decay)
    twice = 2.0 * log_decay
    series = jnp.ones_like(twice)
    for order in range(8, 1, -1):
        series = 1.0 + twice * series * (1.0 / order)
    lost = jnp.where(twice > -0.3, -twice * series, 1.0 - jnp.exp(twice))
    state = jnp.sqrt(lost) * inlet * conv.astype(jnp.float32)
    step = 1
    while step < state.shape[0]:
        state = state + decay * shifted(state, step, 0.0)
        if 2 * step < state.shape[0]:
            decay = decay * shifted(decay, step, 1.0)
        step *= 2
    gelu = 0.5 * gate_in * (
        1.0 + jnp.tanh(0.7978845608028654 * (gate_in + 0.044715 * gate_in * gate_in * gate_in))
    )
    out_ref[...] = (state * gelu).astype(jnp.bfloat16)


def recurrence(tokens, mine, other, meta, taps, rate_blocks, inlet_blocks, plus, shift):
    length, width = tokens.shape
    block = rate_blocks.shape[1]
    blocks = rate_blocks.shape[0]
    parts = [pl.BlockSpec((p.shape[0], block), lambda i: (0, i)) for p in [*mine, *other]]
    column = lambda rows: pl.BlockSpec((rows, block), lambda i: (0, i))
    square = pl.BlockSpec((1, block, block), lambda i: (i, 0, 0))
    return pl.pallas_call(
        functools.partial(recurrence_kernel, len(mine)),
        grid=(blocks,),
        in_specs=[
            pl.BlockSpec(memory_space=pltpu.SMEM),
            pl.BlockSpec((length, width), lambda i: (0, 0)),
            column(taps.shape[0]),
            square,
            square,
            column(1),
            column(length),
            *parts,
        ],
        out_specs=column(length),
        out_shape=jax.ShapeDtypeStruct((length, block * blocks), jnp.bfloat16),
        cost_estimate=pl.CostEstimate(
            flops=4 * length * width * block * blocks,
            bytes_accessed=4 * width * block * blocks + 8 * length * block * blocks,
            transcendentals=0,
        ),
        compiler_params=pltpu.CompilerParams(vmem_limit_bytes=VMEM_BYTES),
    )(meta, tokens, taps, rate_blocks, inlet_blocks, plus, shift, *mine, *other)


def hidden_kernel(count, meta, x_ref, *refs):
    mine, other, out_ref = refs[:count], refs[count : 2 * count], refs[-1]
    first = split_product(meta, x_ref, mine)
    second = split_product(meta, x_ref, other)
    swapped = meta[0] == 1
    gate = jnp.where(swapped, second, first)
    upward = jnp.where(swapped, first, second)
    out_ref[...] = (gate * sigmoid(gate) * upward).astype(jnp.bfloat16)


def hidden_units(normed, mine, other, meta):
    length, width = normed.shape
    units = mine[0].shape[1]
    tile = next(t for t in (512, 640, 256, 128, units) if units % t == 0)
    return pl.pallas_call(
        functools.partial(hidden_kernel, len(mine)),
        grid=(units // tile,),
        in_specs=[
            pl.BlockSpec(memory_space=pltpu.SMEM),
            pl.BlockSpec((length, width), lambda i: (0, 0)),
            *[pl.BlockSpec((p.shape[0], tile), lambda i: (0, i)) for p in [*mine, *other]],
        ],
        out_specs=pl.BlockSpec((length, tile), lambda i: (0, i)),
        out_shape=jax.ShapeDtypeStruct((length, units), jnp.bfloat16),
        cost_estimate=pl.CostEstimate(
            flops=4 * length * width * units, bytes_accessed=4 * width * units, transcendentals=0
        ),
        compiler_params=pltpu.CompilerParams(vmem_limit_bytes=VMEM_BYTES),
    )(meta, normed, *mine, *other)


def outward_kernel(count, meta, left_ref, *refs):
    mine, other, out_ref = refs[:count], refs[count : 2 * count], refs[-1]
    half = mine[0].shape[0]
    near = pl.ds(pl.multiple_of(meta[0] * half, 128), half)
    far = pl.ds(pl.multiple_of((1 - meta[0]) * half, 128), half)
    start = 0
    for at in range(count):
        total = jnp.dot(left_ref[:, near], mine[at][...], preferred_element_type=jnp.float32)
        total += jnp.dot(left_ref[:, far], other[at][...], preferred_element_type=jnp.float32)
        columns = mine[at].shape[1]
        out_ref[:, start : start + columns] = total.astype(jnp.bfloat16)
        start += columns


def outward(left, mine, other, meta):
    length, depth = left.shape
    width = sum(p.shape[1] for p in mine)
    rows = min(length, 256)
    whole = [pl.BlockSpec(p.shape, lambda i: (0, 0)) for p in [*mine, *other]]
    return pl.pallas_call(
        functools.partial(outward_kernel, len(mine)),
        grid=(length // rows,),
        in_specs=[
            pl.BlockSpec(memory_space=pltpu.SMEM),
            pl.BlockSpec((rows, depth), lambda i: (i, 0)),
            *whole,
        ],
        out_specs=pl.BlockSpec((rows, width), lambda i: (i, 0)),
        out_shape=jax.ShapeDtypeStruct((length, width), jnp.bfloat16),
        cost_estimate=pl.CostEstimate(
            flops=2 * length * width * depth, bytes_accessed=2 * width * depth, transcendentals=0
        ),
        compiler_params=pltpu.CompilerParams(vmem_limit_bytes=VMEM_BYTES),
    )(meta, left, *mine, *other)


def add_groups(terms):
    groups = lax.axis_size("tp")
    if groups != 2:
        return lax.psum_scatter(terms, "tp", scatter_dimension=0, tiled=True).astype(jnp.float32)
    share = terms.shape[0] // 2
    me = lax.axis_index("tp")
    away = lax.dynamic_slice_in_dim(terms, (1 - me) * share, share, 0)
    own = lax.dynamic_slice_in_dim(terms, me * share, share, 0)
    came = lax.ppermute(away, "tp", [(0, 1), (1, 0)])
    return own.astype(jnp.float32) + came.astype(jnp.float32)


def grouped_outward(left, mine, other, owners, meta, cut):
    count = len(mine)
    if count == 1:
        return add_groups(outward(left, mine, other, meta))
    outer = count // 2
    chunks = [list(range(count))]
    if cut:
        steps = visit_order(outer)
        last, late = steps[-1], [outer + step for step in steps]
        early = [at for at in range(outer + 1) if at != last]
        chunks = [chunk for chunk in (early, late[:-1], [last], late[-1:]) if chunk]
    width = mine[0].shape[1]
    total = jnp.zeros((left.shape[0] // lax.axis_size("tp"), width * count), jnp.float32)
    for chunk in chunks:
        terms = outward(left, [mine[at] for at in chunk], [other[at] for at in chunk], meta)
        block = add_groups(terms)
        for place, at in enumerate(chunk):
            piece = block[:, place * width : (place + 1) * width]
            total = lax.dynamic_update_slice_in_dim(total, piece, owners[at] * width, 1)
    return total


def all_rows(rows):
    if lax.axis_size("tp") != 2:
        return lax.all_gather(rows, "tp", axis=0, tiled=True)
    came = lax.ppermute(rows, "tp", [(0, 1), (1, 0)])
    low = lax.axis_index("tp") == 0
    return jnp.concatenate([jnp.where(low, rows, came), jnp.where(low, came, rows)], axis=0)


def layer(
    tokens,
    recurrence_branch_weight,
    gate_branch_weight,
    convolution_kernel,
    recurrence_gate_blockwise,
    input_gate_blockwise,
    channel_decay_param,
    token_decay_shift,
    recurrence_output_weight,
    first_norm_gain,
    feedforward_gate_weight,
    feedforward_up_weight,
    feedforward_down_weight,
    second_norm_gain,
):
    share = tokens.shape[0] // lax.axis_size("tp")
    offset = lax.axis_index("tp") * share
    in_mine, in_other, owners, swapped = gather_two(recurrence_branch_weight, gate_branch_weight, 0)
    out_mine, out_other, _, _ = gather_halves(recurrence_output_weight)
    ff_mine, ff_other, _, _ = gather_two(feedforward_gate_weight, feedforward_up_weight, 0)
    down_mine, down_other, _, _ = gather_halves(feedforward_down_weight)
    meta = scalars(owners, swapped)
    branch = recurrence(
        tokens,
        in_mine,
        in_other,
        meta,
        convolution_kernel,
        recurrence_gate_blockwise,
        input_gate_blockwise,
        jax.nn.softplus(-channel_decay_param)[None, :],
        token_decay_shift,
    )
    mix = grouped_outward(branch, out_mine, out_other, owners, meta, False)
    own_tokens = lax.dynamic_slice_in_dim(tokens, offset, share, 0)
    normed = layer_norm(
        residual_scale * own_tokens.astype(jnp.float32) + mix, first_norm_gain
    ).astype(jnp.bfloat16)
    rows = all_rows(normed)
    hidden = hidden_units(rows, ff_mine, ff_other, meta)
    ffn = grouped_outward(hidden, down_mine, down_other, owners, meta, True)
    return layer_norm(residual_scale * normed.astype(jnp.float32) + ffn, second_norm_gain).astype(
        jnp.bfloat16
    )


def solution(mesh):
    return jax.shard_map(
        layer,
        mesh=mesh,
        in_specs=(
            P(("rep", "fs"), None),
            P("fs", "tp"),
            P("fs", "tp"),
            P(None, "tp"),
            P("tp", None, None),
            P("tp", None, None),
            P("tp"),
            P(("rep", "fs"), "tp"),
            P("tp", "fs"),
            P(),
            P("fs", "tp"),
            P("fs", "tp"),
            P("tp", "fs"),
            P(),
        ),
        out_specs=P(("rep", "fs", "tp"), None),
        check_vma=False,
    )
```

profile of v0, /device:TPU:26, one launch (start us, length us, event | category | flops | bytes accessed | tf_op | source)
XLA Modules:
  0.0 530.2 jit_solution(6700288163365061932)
XLA Ops:
  1.9 3.0 collective-permute-start.17
  5.0 1.5 collective-permute-start.18
  7.6 4.6 collective-permute-done.15.refs_1_
  12.2 11.2 %collective-permute-done.16.refs_2_ = bf16[512,256]{1,0:T(8,128)(2,1)S(1)} collective-permute-done((bf16[512,256]{1,0:T(8,128)(2,1)S(1)}, bf16[512,256]{1,0:T(8,128)(2,1)S(1)}, u32[]{:S(2)}, u32[]{:S(2)}) %collective-permute-start.16) | collective-permute-done | bytes 262176 | tf_op jit(solution)/shard_map/ppermute | solution.py:43
  23.5 5.0 collective-permute-start.2
  30.1 4.7 collective-permute-done.refs_1_
  34.7 1.5 collective-permute-start.19
  36.2 25.5 %collective-permute-done.1.refs_2_ = bf16[256,1024]{1,0:T(8,128)(2,1)S(1)} collective-permute-done((bf16[256,1024]{1,0:T(8,128)(2,1)S(1)}, bf16[256,1024]{1,0:T(8,128)(2,1)S(1)}, u32[]{:S(2)}, u32[]{:S(2)}) %collective-permute-start.1) | collective-permute-done | bytes 524320 | tf_op jit(solution)/shard_map/ppermute | solution.py:43
  61.7 1.5 collective-permute-start.20
  63.2 8.8 %collective-permute-done.2.refs_3_ = bf16[256,1024]{1,0:T(8,128)(2,1)S(1)} collective-permute-done((bf16[256,1024]{1,0:T(8,128)(2,1)S(1)}, bf16[256,1024]{1,0:T(8,128)(2,1)S(1)}, u32[]{:S(2)}, u32[]{:S(2)}) %collective-permute-start.2) | collective-permute-done | bytes 524320 | tf_op jit(solution)/shard_map/ppermute | solution.py:43
  74.6 1.5 collective-permute-start.5
  76.1 5.1 collective-permute-done.21.refs_7_
  83.5 9.1 %collective-permute-done.4.refs_5_ = bf16[256,1024]{1,0:T(8,128)(2,1)} collective-permute-done((bf16[256,1024]{1,0:T(8,128)(2,1)S(1)}, bf16[256,1024]{1,0:T(8,128)(2,1)}, u32[]{:S(2)}, u32[]{:S(2)}) %collective-permute-start.4) | collective-permute-done | bytes 524320 | tf_op jit(solution)/shard_map/ppermute | solution.py:46
  92.6 11.2 %collective-permute-done.5.refs_6_ = bf16[256,1024]{1,0:T(8,128)(2,1)} collective-permute-done((bf16[256,1024]{1,0:T(8,128)(2,1)S(1)}, bf16[256,1024]{1,0:T(8,128)(2,1)}, u32[]{:S(2)}, u32[]{:S(2)}) %collective-permute-start.5) | collective-permute-done | bytes 524320 | tf_op jit(solution)/shard_map/ppermute | solution.py:46
  103.8 10.2 %collective-permute-done.6.refs_7_ = bf16[256,1024]{1,0:T(8,128)(2,1)} collective-permute-done((bf16[256,1024]{1,0:T(8,128)(2,1)S(1)}, bf16[256,1024]{1,0:T(8,128)(2,1)}, u32[]{:S(2)}, u32[]{:S(2)}) %collective-permute-start.6) | collective-permute-done | bytes 524320 | tf_op jit(solution)/shard_map/ppermute | solution.py:46
  118.5 17.8 %shard_map.136.left_ref = bf16[512,1024]{1,0:T(8,128)(2,1)} custom-call(s32[9]{0:T(128)} %stack.39.meta, bf16[512,2048]{1,0:T(8,128)(2,1)} %x_ref.1, bf16[4,1024]{1,0:T(4,128)(2,1)} %taps_ref.1, bf16[4,256,256]{2,1,0:T(8,128)(2,1)} %rate_ref.1, bf16[4,256,256]{2,1,0:T(8,128)(2,1)} %inlet_ref.1, f32[1,1024]{1,0:T(1,128)} %bitcast.10, f32[512,1024]{1,0:T(8,128)} %shift_ref.1, ...), custom_call_target="tpu_custom_call" | custom-call | flops 4294967296 | bytes 12582912 | tf_op jit(solution)/shard_map/pallas_call | solution.py:152
  137.1 6.0 %shard_map.137 = bf16[512,2048]{1,0:T(8,128)(2,1)} custom-call(s32[9]{0:T(128)} %stack.39.meta, bf16[512,1024]{1,0:T(8,128)(2,1)} %shard_map.136.left_ref, bf16[512,256]{1,0:T(8,128)(2,1)} %copy-done.18, bf16[512,256]{1,0:T(8,128)(2,1)} %copy-done.33, bf16[512,256]{1,0:T(8,128)(2,1)} %copy-done.34, bf16[512,256]{1,0:T(8,128)(2,1)} %copy-done.35, ...), custom_call_target="tpu_custom_call" | custom-call | flops 2147483648 | bytes 4194304 | tf_op jit(solution)/shard_map/pallas_call | solution.py:226
  143.2 2.4 constant_dynamic-slice_fusion.4
  147.4 2.1 collective-permute-start.32
  149.4 3.4 collective-permute-start.33
  153.0 3.8 collective-permute-start.48
  156.8 14.6 %collective-permute-done.30 = bf16[256,2048]{1,0:T(8,128)(2,1)} collective-permute-done((bf16[256,2048]{1,0:T(8,128)(2,1)}, bf16[256,2048]{1,0:T(8,128)(2,1)}, u32[]{:S(2)}, u32[]{:S(2)}) %collective-permute-start.30) | collective-permute-done | bytes 1048608 | tf_op jit(solution)/shard_map/ppermute | solution.py:251
  171.4 1.6 collective-permute-start.49
  173.0 1.6 convert_add_fusion
  174.9 49.6 %collective-permute-done.47.refs_1_ = bf16[1280,256]{1,0:T(8,128)(2,1)} collective-permute-done((bf16[1280,256]{1,0:T(8,128)(2,1)S(1)}, bf16[1280,256]{1,0:T(8,128)(2,1)}, u32[]{:S(2)}, u32[]{:S(2)}) %collective-permute-start.47) | collective-permute-done | bytes 655392 | tf_op jit(solution)/shard_map/ppermute | solution.py:43
  224.5 10.6 %collective-permute-done.48.refs_2_ = bf16[1280,256]{1,0:T(8,128)(2,1)} collective-permute-done((bf16[1280,256]{1,0:T(8,128)(2,1)S(1)}, bf16[1280,256]{1,0:T(8,128)(2,1)}, u32[]{:S(2)}, u32[]{:S(2)}) %collective-permute-start.48) | collective-permute-done | bytes 655392 | tf_op jit(solution)/shard_map/ppermute | solution.py:43
  235.1 57.8 %collective-permute-start.60 = (bf16[1280,256]{1,0:T(8,128)(2,1)S(1)}, bf16[1280,256]{1,0:T(8,128)(2,1)S(1)}, u32[]{:S(2)}, u32[]{:S(2)}) collective-permute-start(bf16[1280,256]{1,0:T(8,128)(2,1)S(1)} %slice_select_fusion.refs_0_), channel_id=1, source_target_pairs={{0,8},{2,10},{4,12},{6,14},{8,0},{10,2},{12,4},{14,6},{1,9},{3,11}... | collective-permute-start | bytes 1966088 | tf_op jit(solution)/shard_map/ppermute | solution.py:43
  293.0 1.6 collective-permute-start.35
  294.6 54.9 %collective-permute-done.60.refs_0_ = bf16[1280,256]{1,0:T(8,128)(2,1)S(1)} collective-permute-done((bf16[1280,256]{1,0:T(8,128)(2,1)S(1)}, bf16[1280,256]{1,0:T(8,128)(2,1)S(1)}, u32[]{:S(2)}, u32[]{:S(2)}) %collective-permute-start.60) | collective-permute-done | bytes 655392 | tf_op jit(solution)/shard_map/ppermute | solution.py:43
  349.5 1.6 collective-permute-start.55
  351.7 1.6 collective-permute-start.36
  353.6 13.8 %collective-permute-done.55.refs_0_ = bf16[1280,256]{1,0:T(8,128)(2,1)S(1)} collective-permute-done((bf16[1280,256]{1,0:T(8,128)(2,1)}, bf16[1280,256]{1,0:T(8,128)(2,1)S(1)}, u32[]{:S(2)}, u32[]{:S(2)}) %collective-permute-start.55) | collective-permute-done | bytes 655392 | tf_op jit(solution)/shard_map/ppermute | solution.py:46
  367.4 14.0 %collective-permute-done.56.refs_1_ = bf16[1280,256]{1,0:T(8,128)(2,1)S(1)} collective-permute-done((bf16[1280,256]{1,0:T(8,128)(2,1)}, bf16[1280,256]{1,0:T(8,128)(2,1)S(1)}, u32[]{:S(2)}, u32[]{:S(2)}) %collective-permute-start.56) | collective-permute-done | bytes 655392 | tf_op jit(solution)/shard_map/ppermute | solution.py:46
  385.9 23.7 %collective-permute-done.36.refs_5_ = bf16[256,2560]{1,0:T(8,128)(2,1)} collective-permute-done((bf16[256,2560]{1,0:T(8,128)(2,1)}, bf16[256,2560]{1,0:T(8,128)(2,1)}, u32[]{:S(2)}, u32[]{:S(2)}) %collective-permute-start.36) | collective-permute-done | bytes 1310752 | tf_op jit(solution)/shard_map/ppermute | solution.py:46
  411.1 26.6 %collective-permute-done.37.refs_6_ = bf16[256,2560]{1,0:T(8,128)(2,1)} collective-permute-done((bf16[256,2560]{1,0:T(8,128)(2,1)}, bf16[256,2560]{1,0:T(8,128)(2,1)}, u32[]{:S(2)}, u32[]{:S(2)}) %collective-permute-start.37) | collective-permute-done | bytes 1310752 | tf_op jit(solution)/shard_map/ppermute | solution.py:46
  437.7 27.6 %collective-permute-done.38.refs_7_ = bf16[256,2560]{1,0:T(8,128)(2,1)} collective-permute-done((bf16[256,2560]{1,0:T(8,128)(2,1)}, bf16[256,2560]{1,0:T(8,128)(2,1)}, u32[]{:S(2)}, u32[]{:S(2)}) %collective-permute-start.38) | collective-permute-done | bytes 1310752 | tf_op jit(solution)/shard_map/ppermute | solution.py:46
  467.4 1.6 pad_maximum_fusion.x_ref
  470.7 1.7 collective-permute-done.45.refs_14_
  474.4 16.8 %shard_map.138.left_ref = bf16[512,2560]{1,0:T(8,128)(2,1)} custom-call(s32[9]{0:T(128)} %stack.39.meta, bf16[512,2048]{1,0:T(8,128)(2,1)} %pad_maximum_fusion.x_ref, bf16[256,2560]{1,0:T(8,128)(2,1)} %broadcast_select_fusion.refs_0_, bf16[256,2560]{1,0:T(8,128)(2,1)} %collective-permute-done.32.refs_1_, bf16[256,2560]{1,0:T(8,128)(2,1)} %collective-permute-done.33.refs_2_, ...), custom_call_target="tpu_custom_call" | custom-call | flops 10737418240 | bytes 20971520 | tf_op jit(solution)/shard_map/pallas_call | solution.py:190
  491.2 4.5 shard_map.140
  496.2 1.7 constant_dynamic-slice_fusion.2
  499.4 6.8 %shard_map.139 = bf16[512,1024]{1,0:T(8,128)(2,1)} custom-call(s32[9]{0:T(128)} %stack.39.meta, bf16[512,2560]{1,0:T(8,128)(2,1)} %shard_map.138.left_ref, bf16[1280,256]{1,0:T(8,128)(2,1)} %copy-done.16, bf16[1280,256]{1,0:T(8,128)(2,1)} %collective-permute-done.47.refs_1_, bf16[1280,256]{1,0:T(8,128)(2,1)} %collective-permute-done.48.refs_2_, ...), custom_call_target="tpu_custom_call" | custom-call | flops 2684354560 | bytes 5242880 | tf_op jit(solution)/shard_map/pallas_call | solution.py:226
  506.1 1.9 constant_dynamic-slice_fusion.3
  509.5 3.4 shard_map.141
  513.8 1.6 collective-permute-start.62
  515.4 3.4 shard_map.142
  521.3 1.8 collective-permute-done.54
  525.9 1.7 collective-permute-done.65
  (225 shorter events, 41.5 us)
Async XLA Ops:
  1.6 21.9 %collective-permute-start.16 = (bf16[512,256]{1,0:T(8,128)(2,1)S(1)}, bf16[512,256]{1,0:T(8,128)(2,1)S(1)}, u32[]{:S(2)}, u32[]{:S(2)}) collective-permute-start(bf16[512,256]{1,0:T(8,128)(2,1)S(1)} %slice_select_fusion.1.refs_0_), channel_id=1, source_target_pairs={{0,8},{2,10},{4,12},{6,14},{8,0},{10,2},{12,4},{14,6},{1,9},{3,11}... | collective-permute-start | bytes 786440 | tf_op jit(solution)/shard_map/ppermute | solution.py:43
  1.9 21.5 %collective-permute-start.17 = (bf16[512,256]{1,0:T(8,128)(2,1)S(1)}, bf16[512,256]{1,0:T(8,128)(2,1)S(1)}, u32[]{:S(2)}, u32[]{:S(2)}) collective-permute-start(bf16[512,256]{1,0:T(8,128)(2,1)S(1)} %slice_select_fusion.1.refs_0_), channel_id=1, source_target_pairs={{0,4},{2,6},{4,8},{6,10},{8,12},{10,14},{12,0},{14,2},{1,5},{3,7},... | collective-permute-start | bytes 786440 | tf_op jit(solution)/shard_map/ppermute | solution.py:43
  5.0 23.6 %collective-permute-start.18 = (bf16[512,256]{1,0:T(8,128)(2,1)S(1)}, bf16[512,256]{1,0:T(8,128)(2,1)S(1)}, u32[]{:S(2)}, u32[]{:S(2)}) collective-permute-start(bf16[512,256]{1,0:T(8,128)(2,1)S(1)} %slice_select_fusion.1.refs_0_), channel_id=1, source_target_pairs={{0,2},{2,0},{4,6},{6,4},{8,10},{10,8},{12,14},{14,12},{1,3},{3,1},... | collective-permute-start | bytes 786440 | tf_op jit(solution)/shard_map/ppermute | solution.py:46
  6.5 23.6 %collective-permute-start.22 = (bf16[512,256]{1,0:T(8,128)(2,1)S(1)}, bf16[512,256]{1,0:T(8,128)(2,1)S(1)}, u32[]{:S(2)}, u32[]{:S(2)}) collective-permute-start(bf16[512,256]{1,0:T(8,128)(2,1)S(1)} %slice_select_fusion.1.refs_0_), channel_id=1, source_target_pairs={{0,16},{16,0},{1,17},{17,1},{2,18},{18,2},{3,19},{19,3},{4,20},{20... | collective-permute-start | bytes 786440 | tf_op jit(solution)/shard_map/ppermute | solution.py:50
  12.2 22.5 %collective-permute-start = (bf16[256,1024]{1,0:T(8,128)(2,1)S(1)}, bf16[256,1024]{1,0:T(8,128)(2,1)S(1)}, u32[]{:S(2)}, u32[]{:S(2)}) collective-permute-start(bf16[256,1024]{1,0:T(8,128)(2,1)S(1)} %broadcast_select_fusion.3.refs_0_), channel_id=1, source_target_pairs={{0,12},{2,14},{4,0},{6,2},{8,4},{10,6},{12,8},{14,10},{1,13},{3,15... | collective-permute-start | bytes 1572872 | tf_op jit(solution)/shard_map/ppermute | solution.py:43
  23.5 38.3 %collective-permute-start.1 = (bf16[256,1024]{1,0:T(8,128)(2,1)S(1)}, bf16[256,1024]{1,0:T(8,128)(2,1)S(1)}, u32[]{:S(2)}, u32[]{:S(2)}) collective-permute-start(bf16[256,1024]{1,0:T(8,128)(2,1)S(1)} %broadcast_select_fusion.3.refs_0_), channel_id=1, source_target_pairs={{0,8},{2,10},{4,12},{6,14},{8,0},{10,2},{12,4},{14,6},{1,9},{3,11}... | collective-permute-start | bytes 1572872 | tf_op jit(solution)/shard_map/ppermute | solution.py:43
  23.5 48.6 %collective-permute-start.2 = (bf16[256,1024]{1,0:T(8,128)(2,1)S(1)}, bf16[256,1024]{1,0:T(8,128)(2,1)S(1)}, u32[]{:S(2)}, u32[]{:S(2)}) collective-permute-start(bf16[256,1024]{1,0:T(8,128)(2,1)S(1)} %broadcast_select_fusion.3.refs_0_), channel_id=1, source_target_pairs={{0,4},{2,6},{4,8},{6,10},{8,12},{10,14},{12,0},{14,2},{1,5},{3,7},... | collective-permute-start | bytes 1572872 | tf_op jit(solution)/shard_map/ppermute | solution.py:43
  28.5 45.0 %collective-permute-start.3 = (bf16[256,1024]{1,0:T(8,128)(2,1)S(1)}, bf16[256,1024]{1,0:T(8,128)(2,1)S(1)}, u32[]{:S(2)}, u32[]{:S(2)}) collective-permute-start(bf16[256,1024]{1,0:T(8,128)(2,1)S(1)} %broadcast_select_fusion.3.refs_0_), channel_id=1, source_target_pairs={{0,2},{2,0},{4,6},{6,4},{8,10},{10,8},{12,14},{14,12},{1,3},{3,1},... | collective-permute-start | bytes 1572872 | tf_op jit(solution)/shard_map/ppermute | solution.py:46
  30.0 43.5 %collective-permute-start.7 = (bf16[256,1024]{1,0:T(8,128)(2,1)S(1)}, bf16[256,1024]{1,0:T(8,128)(2,1)S(1)}, u32[]{:S(2)}, u32[]{:S(2)}) collective-permute-start(bf16[256,1024]{1,0:T(8,128)(2,1)S(1)} %broadcast_select_fusion.3.refs_0_), channel_id=1, source_target_pairs={{0,16},{16,0},{1,17},{17,1},{2,18},{18,2},{3,19},{19,3},{4,20},{20... | collective-permute-start | bytes 1572872 | tf_op jit(solution)/shard_map/ppermute | solution.py:50
  34.7 39.4 %collective-permute-start.19 = (bf16[512,256]{1,0:T(8,128)(2,1)S(1)}, bf16[512,256]{1,0:T(8,128)(2,1)S(1)}, u32[]{:S(2)}, u32[]{:S(2)}) collective-permute-start(bf16[512,256]{1,0:T(8,128)(2,1)S(1)} %collective-permute-done.15.refs_1_), channel_id=1, source_target_pairs={{0,2},{2,0},{4,6},{6,4},{8,10},{10,8},{12,14},{14,12},{1,3},{3,1},... | collective-permute-start | bytes 786440 | tf_op jit(solution)/shard_map/ppermute | solution.py:46
  74.1 18.5 %collective-permute-start.4 = (bf16[256,1024]{1,0:T(8,128)(2,1)S(1)}, bf16[256,1024]{1,0:T(8,128)(2,1)}, u32[]{:S(2)}, u32[]{:S(2)}) collective-permute-start(bf16[256,1024]{1,0:T(8,128)(2,1)S(1)} %collective-permute-done.refs_1_), channel_id=1, source_target_pairs={{0,2},{2,0},{4,6},{6,4},{8,10},{10,8},{12,14},{14,12},{1,3},{3,1},... | collective-permute-start | bytes 1572872 | tf_op jit(solution)/shard_map/ppermute | solution.py:46
  74.6 29.2 %collective-permute-start.5 = (bf16[256,1024]{1,0:T(8,128)(2,1)S(1)}, bf16[256,1024]{1,0:T(8,128)(2,1)}, u32[]{:S(2)}, u32[]{:S(2)}) collective-permute-start(bf16[256,1024]{1,0:T(8,128)(2,1)S(1)} %collective-permute-done.1.refs_2_), channel_id=1, source_target_pairs={{0,2},{2,0},{4,6},{6,4},{8,10},{10,8},{12,14},{14,12},{1,3},{3,1},... | collective-permute-start | bytes 1572872 | tf_op jit(solution)/shard_map/ppermute | solution.py:46
  81.2 32.8 %collective-permute-start.6 = (bf16[256,1024]{1,0:T(8,128)(2,1)S(1)}, bf16[256,1024]{1,0:T(8,128)(2,1)}, u32[]{:S(2)}, u32[]{:S(2)}) collective-permute-start(bf16[256,1024]{1,0:T(8,128)(2,1)S(1)} %collective-permute-done.2.refs_3_), channel_id=1, source_target_pairs={{0,2},{2,0},{4,6},{6,4},{8,10},{10,8},{12,14},{14,12},{1,3},{3,1},... | collective-permute-start | bytes 1572872 | tf_op jit(solution)/shard_map/ppermute | solution.py:46
  82.8 31.3 %collective-permute-start.10 = (bf16[256,1024]{1,0:T(8,128)(2,1)S(1)}, bf16[256,1024]{1,0:T(8,128)(2,1)S(1)}, u32[]{:S(2)}, u32[]{:S(2)}) collective-permute-start(bf16[256,1024]{1,0:T(8,128)(2,1)S(1)} %collective-permute-done.2.refs_3_), channel_id=1, source_target_pairs={{0,16},{16,0},{1,17},{17,1},{2,18},{18,2},{3,19},{19,3},{4,20},{20... | collective-permute-start | bytes 1572872 | tf_op jit(solution)/shard_map/ppermute | solution.py:50
  83.4 31.1 %collective-permute-start.8 = (bf16[256,1024]{1,0:T(8,128)(2,1)S(1)}, bf16[256,1024]{1,0:T(8,128)(2,1)S(1)}, u32[]{:S(2)}, u32[]{:S(2)}) collective-permute-start(bf16[256,1024]{1,0:T(8,128)(2,1)S(1)} %collective-permute-done.refs_1_), channel_id=1, source_target_pairs={{0,16},{16,0},{1,17},{17,1},{2,18},{18,2},{3,19},{19,3},{4,20},{20... | collective-permute-start | bytes 1572872 | tf_op jit(solution)/shard_map/ppermute | solution.py:50
  92.6 24.8 %collective-permute-start.9 = (bf16[256,1024]{1,0:T(8,128)(2,1)S(1)}, bf16[256,1024]{1,0:T(8,128)(2,1)}, u32[]{:S(2)}, u32[]{:S(2)}) collective-permute-start(bf16[256,1024]{1,0:T(8,128)(2,1)S(1)} %collective-permute-done.1.refs_2_), channel_id=1, source_target_pairs={{0,16},{16,0},{1,17},{17,1},{2,18},{18,2},{3,19},{19,3},{4,20},{20... | collective-permute-start | bytes 1572872 | tf_op jit(solution)/shard_map/ppermute | solution.py:50
  117.4 19.0 %collective-permute-start.25 = (bf16[512,256]{1,0:T(8,128)(2,1)}, bf16[512,256]{1,0:T(8,128)(2,1)S(1)}, u32[]{:S(2)}, u32[]{:S(2)}) collective-permute-start(bf16[512,256]{1,0:T(8,128)(2,1)} %copy-done.35), channel_id=1, source_target_pairs={{0,16},{16,0},{1,17},{17,1},{2,18},{18,2},{3,19},{19,3},{4,20},{20... | collective-permute-start | bytes 786440 | tf_op jit(solution)/shard_map/ppermute | solution.py:50
  117.4 19.0 %collective-permute-start.26 = (bf16[512,256]{1,0:T(8,128)(2,1)}, bf16[512,256]{1,0:T(8,128)(2,1)S(1)}, u32[]{:S(2)}, u32[]{:S(2)}) collective-permute-start(bf16[512,256]{1,0:T(8,128)(2,1)} %copy-done.36), channel_id=1, source_target_pairs={{0,16},{16,0},{1,17},{17,1},{2,18},{18,2},{3,19},{19,3},{4,20},{20... | collective-permute-start | bytes 786440 | tf_op jit(solution)/shard_map/ppermute | solution.py:50
  117.9 18.5 %collective-permute-start.27 = (bf16[512,256]{1,0:T(8,128)(2,1)}, bf16[512,256]{1,0:T(8,128)(2,1)}, u32[]{:S(2)}, u32[]{:S(2)}) collective-permute-start(bf16[512,256]{1,0:T(8,128)(2,1)} %copy-done.38), channel_id=1, source_target_pairs={{0,16},{16,0},{1,17},{17,1},{2,18},{18,2},{3,19},{19,3},{4,20},{20... | collective-permute-start | bytes 786440 | tf_op jit(solution)/shard_map/ppermute | solution.py:50
  118.0 18.4 %collective-permute-start.28 = (bf16[512,256]{1,0:T(8,128)(2,1)}, bf16[512,256]{1,0:T(8,128)(2,1)}, u32[]{:S(2)}, u32[]{:S(2)}) collective-permute-start(bf16[512,256]{1,0:T(8,128)(2,1)} %copy-done.39), channel_id=1, source_target_pairs={{0,16},{16,0},{1,17},{17,1},{2,18},{18,2},{3,19},{19,3},{4,20},{20... | collective-permute-start | bytes 786440 | tf_op jit(solution)/shard_map/ppermute | solution.py:50
  118.4 18.0 %collective-permute-start.29 = (bf16[512,256]{1,0:T(8,128)(2,1)}, bf16[512,256]{1,0:T(8,128)(2,1)}, u32[]{:S(2)}, u32[]{:S(2)}) collective-permute-start(bf16[512,256]{1,0:T(8,128)(2,1)} %copy-done.40), channel_id=1, source_target_pairs={{0,16},{16,0},{1,17},{17,1},{2,18},{18,2},{3,19},{19,3},{4,20},{20... | collective-permute-start | bytes 786440 | tf_op jit(solution)/shard_map/ppermute | solution.py:50
  145.6 25.8 %collective-permute-start.30 = (bf16[256,2048]{1,0:T(8,128)(2,1)}, bf16[256,2048]{1,0:T(8,128)(2,1)}, u32[]{:S(2)}, u32[]{:S(2)}) collective-permute-start(bf16[256,2048]{1,0:T(8,128)(2,1)} %constant_dynamic-slice_fusion.4), channel_id=1, source_target_pairs={{0,1},{1,0},{2,3},{3,2},{4,5},{5,4},{6,7},{7,6},{8,9},{9,8},{10,11... | collective-permute-start | bytes 3145736 | tf_op jit(solution)/shard_map/ppermute | solution.py:251
  147.4 202.1 %collective-permute-start.32 = (bf16[256,2560]{1,0:T(8,128)(2,1)}, bf16[256,2560]{1,0:T(8,128)(2,1)}, u32[]{:S(2)}, u32[]{:S(2)}) collective-permute-start(bf16[256,2560]{1,0:T(8,128)(2,1)} %broadcast_select_fusion.refs_0_), channel_id=1, source_target_pairs={{0,12},{2,14},{4,0},{6,2},{8,4},{10,6},{12,8},{14,10},{1,13},{3,15... | collective-permute-start | bytes 3932168 | tf_op jit(solution)/shard_map/ppermute | solution.py:43
  149.4 201.6 %collective-permute-start.33 = (bf16[256,2560]{1,0:T(8,128)(2,1)}, bf16[256,2560]{1,0:T(8,128)(2,1)}, u32[]{:S(2)}, u32[]{:S(2)}) collective-permute-start(bf16[256,2560]{1,0:T(8,128)(2,1)} %broadcast_select_fusion.refs_0_), channel_id=1, source_target_pairs={{0,8},{2,10},{4,12},{6,14},{8,0},{10,2},{12,4},{14,6},{1,9},{3,11}... | collective-permute-start | bytes 3932168 | tf_op jit(solution)/shard_map/ppermute | solution.py:43
  152.9 71.5 %collective-permute-start.47 = (bf16[1280,256]{1,0:T(8,128)(2,1)S(1)}, bf16[1280,256]{1,0:T(8,128)(2,1)}, u32[]{:S(2)}, u32[]{:S(2)}) collective-permute-start(bf16[1280,256]{1,0:T(8,128)(2,1)S(1)} %slice_select_fusion.refs_0_), channel_id=1, source_target_pairs={{0,12},{2,14},{4,0},{6,2},{8,4},{10,6},{12,8},{14,10},{1,13},{3,15... | collective-permute-start | bytes 1966088 | tf_op jit(solution)/shard_map/ppermute | solution.py:43
  153.0 82.1 %collective-permute-start.48 = (bf16[1280,256]{1,0:T(8,128)(2,1)S(1)}, bf16[1280,256]{1,0:T(8,128)(2,1)}, u32[]{:S(2)}, u32[]{:S(2)}) collective-permute-start(bf16[1280,256]{1,0:T(8,128)(2,1)S(1)} %slice_select_fusion.refs_0_), channel_id=1, source_target_pairs={{0,4},{2,6},{4,8},{6,10},{8,12},{10,14},{12,0},{14,2},{1,5},{3,7},... | collective-permute-start | bytes 1966088 | tf_op jit(solution)/shard_map/ppermute | solution.py:43
  171.4 63.7 %collective-permute-start.49 = (bf16[1280,256]{1,0:T(8,128)(2,1)S(1)}, bf16[1280,256]{1,0:T(8,128)(2,1)}, u32[]{:S(2)}, u32[]{:S(2)}) collective-permute-start(bf16[1280,256]{1,0:T(8,128)(2,1)S(1)} %slice_select_fusion.refs_0_), channel_id=1, source_target_pairs={{0,2},{2,0},{4,6},{6,4},{8,10},{10,8},{12,14},{14,12},{1,3},{3,1},... | collective-permute-start | bytes 1966088 | tf_op jit(solution)/shard_map/ppermute | solution.py:46
  224.4 127.2 %collective-permute-start.34 = (bf16[256,2560]{1,0:T(8,128)(2,1)}, bf16[256,2560]{1,0:T(8,128)(2,1)}, u32[]{:S(2)}, u32[]{:S(2)}) collective-permute-start(bf16[256,2560]{1,0:T(8,128)(2,1)} %broadcast_select_fusion.refs_0_), channel_id=1, source_target_pairs={{0,4},{2,6},{4,8},{6,10},{8,12},{10,14},{12,0},{14,2},{1,5},{3,7},... | collective-permute-start | bytes 3932168 | tf_op jit(solution)/shard_map/ppermute | solution.py:43
  235.1 57.9 %collective-permute-start.50 = (bf16[1280,256]{1,0:T(8,128)(2,1)S(1)}, bf16[1280,256]{1,0:T(8,128)(2,1)S(1)}, u32[]{:S(2)}, u32[]{:S(2)}) collective-permute-start(bf16[1280,256]{1,0:T(8,128)(2,1)S(1)} %slice_select_fusion.refs_0_), channel_id=1, source_target_pairs={{0,16},{16,0},{1,17},{17,1},{2,18},{18,2},{3,19},{19,3},{4,20},{20... | collective-permute-start | bytes 1966088 | tf_op jit(solution)/shard_map/ppermute | solution.py:50
  235.1 114.4 %collective-permute-start.60 = (bf16[1280,256]{1,0:T(8,128)(2,1)S(1)}, bf16[1280,256]{1,0:T(8,128)(2,1)S(1)}, u32[]{:S(2)}, u32[]{:S(2)}) collective-permute-start(bf16[1280,256]{1,0:T(8,128)(2,1)S(1)} %slice_select_fusion.refs_0_), channel_id=1, source_target_pairs={{0,8},{2,10},{4,12},{6,14},{8,0},{10,2},{12,4},{14,6},{1,9},{3,11}... | collective-permute-start | bytes 1966088 | tf_op jit(solution)/shard_map/ppermute | solution.py:43
  293.0 88.9 %collective-permute-start.35 = (bf16[256,2560]{1,0:T(8,128)(2,1)}, bf16[256,2560]{1,0:T(8,128)(2,1)}, u32[]{:S(2)}, u32[]{:S(2)}) collective-permute-start(bf16[256,2560]{1,0:T(8,128)(2,1)} %broadcast_select_fusion.refs_0_), channel_id=1, source_target_pairs={{0,2},{2,0},{4,6},{6,4},{8,10},{10,8},{12,14},{14,12},{1,3},{3,1},... | collective-permute-start | bytes 3932168 | tf_op jit(solution)/shard_map/ppermute | solution.py:46
  349.5 33.0 %collective-permute-start.39 = (bf16[256,2560]{1,0:T(8,128)(2,1)}, bf16[256,2560]{1,0:T(8,128)(2,1)S(1)}, u32[]{:S(2)}, u32[]{:S(2)}) collective-permute-start(bf16[256,2560]{1,0:T(8,128)(2,1)} %broadcast_select_fusion.refs_0_), channel_id=1, source_target_pairs={{0,16},{16,0},{1,17},{17,1},{2,18},{18,2},{3,19},{19,3},{4,20},{20... | collective-permute-start | bytes 3932168 | tf_op jit(solution)/shard_map/ppermute | solution.py:50
  349.5 17.9 %collective-permute-start.55 = (bf16[1280,256]{1,0:T(8,128)(2,1)}, bf16[1280,256]{1,0:T(8,128)(2,1)S(1)}, u32[]{:S(2)}, u32[]{:S(2)}) collective-permute-start(bf16[1280,256]{1,0:T(8,128)(2,1)} %collective-permute-done.47.refs_1_), channel_id=1, source_target_pairs={{0,2},{2,0},{4,6},{6,4},{8,10},{10,8},{12,14},{14,12},{1,3},{3,1},... | collective-permute-start | bytes 1966088 | tf_op jit(solution)/shard_map/ppermute | solution.py:46
  351.1 30.3 %collective-permute-start.56 = (bf16[1280,256]{1,0:T(8,128)(2,1)}, bf16[1280,256]{1,0:T(8,128)(2,1)S(1)}, u32[]{:S(2)}, u32[]{:S(2)}) collective-permute-start(bf16[1280,256]{1,0:T(8,128)(2,1)} %collective-permute-done.48.refs_2_), channel_id=1, source_target_pairs={{0,2},{2,0},{4,6},{6,4},{8,10},{10,8},{12,14},{14,12},{1,3},{3,1},... | collective-permute-start | bytes 1966088 | tf_op jit(solution)/shard_map/ppermute | solution.py:46
  351.7 57.9 %collective-permute-start.36 = (bf16[256,2560]{1,0:T(8,128)(2,1)}, bf16[256,2560]{1,0:T(8,128)(2,1)}, u32[]{:S(2)}, u32[]{:S(2)}) collective-permute-start(bf16[256,2560]{1,0:T(8,128)(2,1)} %collective-permute-done.32.refs_1_), channel_id=1, source_target_pairs={{0,2},{2,0},{4,6},{6,4},{8,10},{10,8},{12,14},{14,12},{1,3},{3,1},... | collective-permute-start | bytes 3932168 | tf_op jit(solution)/shard_map/ppermute | solution.py:46
  382.0 83.3 %collective-permute-start.40 = (bf16[256,2560]{1,0:T(8,128)(2,1)}, bf16[256,2560]{1,0:T(8,128)(2,1)S(1)}, u32[]{:S(2)}, u32[]{:S(2)}) collective-permute-start(bf16[256,2560]{1,0:T(8,128)(2,1)} %collective-permute-done.32.refs_1_), channel_id=1, source_target_pairs={{0,16},{16,0},{1,17},{17,1},{2,18},{18,2},{3,19},{19,3},{4,20},{20... | collective-permute-start | bytes 3932168 | tf_op jit(solution)/shard_map/ppermute | solution.py:50
  382.5 55.2 %collective-permute-start.37 = (bf16[256,2560]{1,0:T(8,128)(2,1)}, bf16[256,2560]{1,0:T(8,128)(2,1)}, u32[]{:S(2)}, u32[]{:S(2)}) collective-permute-start(bf16[256,2560]{1,0:T(8,128)(2,1)} %collective-permute-done.33.refs_2_), channel_id=1, source_target_pairs={{0,2},{2,0},{4,6},{6,4},{8,10},{10,8},{12,14},{14,12},{1,3},{3,1},... | collective-permute-start | bytes 3932168 | tf_op jit(solution)/shard_map/ppermute | solution.py:46
  384.0 81.7 %collective-permute-start.41 = (bf16[256,2560]{1,0:T(8,128)(2,1)}, bf16[256,2560]{1,0:T(8,128)(2,1)S(1)}, u32[]{:S(2)}, u32[]{:S(2)}) collective-permute-start(bf16[256,2560]{1,0:T(8,128)(2,1)} %collective-permute-done.33.refs_2_), channel_id=1, source_target_pairs={{0,16},{16,0},{1,17},{17,1},{2,18},{18,2},{3,19},{19,3},{4,20},{20... | collective-permute-start | bytes 3932168 | tf_op jit(solution)/shard_map/ppermute | solution.py:50
  384.9 80.4 %collective-permute-start.38 = (bf16[256,2560]{1,0:T(8,128)(2,1)}, bf16[256,2560]{1,0:T(8,128)(2,1)}, u32[]{:S(2)}, u32[]{:S(2)}) collective-permute-start(bf16[256,2560]{1,0:T(8,128)(2,1)} %collective-permute-done.34.refs_3_), channel_id=1, source_target_pairs={{0,2},{2,0},{4,6},{6,4},{8,10},{10,8},{12,14},{14,12},{1,3},{3,1},... | collective-permute-start | bytes 3932168 | tf_op jit(solution)/shard_map/ppermute | solution.py:46
  409.6 56.3 %collective-permute-start.31 = (bf16[256,2048]{1,0:T(8,128)(2,1)S(1)}, bf16[256,2048]{1,0:T(8,128)(2,1)S(1)}, u32[]{:S(2)}, u32[]{:S(2)}) collective-permute-start(bf16[256,2048]{1,0:T(8,128)(2,1)S(1)} %multiply_convert_fusion.1), channel_id=1, source_target_pairs={{0,1},{1,0},{2,3},{3,2},{4,5},{5,4},{6,7},{7,6},{8,9},{9,8},{10,11... | collective-permute-start | bytes 3145736 | tf_op jit(solution)/shard_map/ppermute | solution.py:280
  437.7 31.3 %collective-permute-start.42 = (bf16[256,2560]{1,0:T(8,128)(2,1)}, bf16[256,2560]{1,0:T(8,128)(2,1)}, u32[]{:S(2)}, u32[]{:S(2)}) collective-permute-start(bf16[256,2560]{1,0:T(8,128)(2,1)} %collective-permute-done.34.refs_3_), channel_id=1, source_target_pairs={{0,16},{16,0},{1,17},{17,1},{2,18},{18,2},{3,19},{19,3},{4,20},{20... | collective-permute-start | bytes 3932168 | tf_op jit(solution)/shard_map/ppermute | solution.py:50
  469.0 28.9 %collective-permute-start.51 = (bf16[1280,256]{1,0:T(8,128)(2,1)}, bf16[1280,256]{1,0:T(8,128)(2,1)}, u32[]{:S(2)}, u32[]{:S(2)}) collective-permute-start(bf16[1280,256]{1,0:T(8,128)(2,1)} %collective-permute-done.47.refs_1_), channel_id=1, source_target_pairs={{0,16},{16,0},{1,17},{17,1},{2,18},{18,2},{3,19},{19,3},{4,20},{20... | collective-permute-start | bytes 1966088 | tf_op jit(solution)/shard_map/ppermute | solution.py:50
  469.1 30.3 %collective-permute-start.52 = (bf16[1280,256]{1,0:T(8,128)(2,1)}, bf16[1280,256]{1,0:T(8,128)(2,1)}, u32[]{:S(2)}, u32[]{:S(2)}) collective-permute-start(bf16[1280,256]{1,0:T(8,128)(2,1)} %collective-permute-done.48.refs_2_), channel_id=1, source_target_pairs={{0,16},{16,0},{1,17},{17,1},{2,18},{18,2},{3,19},{19,3},{4,20},{20... | collective-permute-start | bytes 1966088 | tf_op jit(solution)/shard_map/ppermute | solution.py:50
  470.5 38.0 %collective-permute-start.61 = (bf16[1280,256]{1,0:T(8,128)(2,1)S(1)}, bf16[1280,256]{1,0:T(8,128)(2,1)S(1)}, u32[]{:S(2)}, u32[]{:S(2)}) collective-permute-start(bf16[1280,256]{1,0:T(8,128)(2,1)S(1)} %collective-permute-done.60.refs_0_), channel_id=1, source_target_pairs={{0,16},{16,0},{1,17},{17,1},{2,18},{18,2},{3,19},{19,3},{4,20},{20... | collective-permute-start | bytes 1966088 | tf_op jit(solution)/shard_map/ppermute | solution.py:50
  472.4 23.4 %collective-permute-start.63 = (bf16[1280,256]{1,0:T(8,128)(2,1)S(1)}, bf16[1280,256]{1,0:T(8,128)(2,1)S(1)}, u32[]{:S(2)}, u32[]{:S(2)}) collective-permute-start(bf16[1280,256]{1,0:T(8,128)(2,1)S(1)} %collective-permute-done.60.refs_0_), channel_id=1, source_target_pairs={{0,2},{2,0},{4,6},{6,4},{8,10},{10,8},{12,14},{14,12},{1,3},{3,1},... | collective-permute-start | bytes 1966088 | tf_op jit(solution)/shard_map/ppermute | solution.py:46
  474.3 25.1 %collective-permute-start.53 = (bf16[1280,256]{1,0:T(8,128)(2,1)}, bf16[1280,256]{1,0:T(8,128)(2,1)}, u32[]{:S(2)}, u32[]{:S(2)}) collective-permute-start(bf16[1280,256]{1,0:T(8,128)(2,1)} %collective-permute-done.49.refs_3_), channel_id=1, source_target_pairs={{0,16},{16,0},{1,17},{17,1},{2,18},{18,2},{3,19},{19,3},{4,20},{20... | collective-permute-start | bytes 1966088 | tf_op jit(solution)/shard_map/ppermute | solution.py:50
  495.8 19.6 %collective-permute-start.64 = (bf16[1280,256]{1,0:T(8,128)(2,1)S(1)}, bf16[1280,256]{1,0:T(8,128)(2,1)}, u32[]{:S(2)}, u32[]{:S(2)}) collective-permute-start(bf16[1280,256]{1,0:T(8,128)(2,1)S(1)} %collective-permute-done.63.refs_0_), channel_id=1, source_target_pairs={{0,16},{16,0},{1,17},{17,1},{2,18},{18,2},{3,19},{19,3},{4,20},{20... | collective-permute-start | bytes 1966088 | tf_op jit(solution)/shard_map/ppermute | solution.py:50
  497.9 22.4 %collective-permute-start.59 = (bf16[256,512]{1,0:T(8,128)(2,1)}, bf16[256,512]{1,0:T(8,128)(2,1)}, u32[]{:S(2)}, u32[]{:S(2)}) collective-permute-start(bf16[256,512]{1,0:T(8,128)(2,1)} %constant_dynamic-slice_fusion.2), channel_id=1, source_target_pairs={{0,1},{1,0},{2,3},{3,2},{4,5},{5,4},{6,7},{7,6},{8,9},{9,8},{10,11... | collective-permute-start | bytes 786440 | tf_op jit(solution)/shard_map/ppermute | solution.py:251
  (63 other events, 1963.0 us)
where the time goes:
time: 531 us; the launch traced here: 530 us
  waiting for transfers between devices  334 us (63%)
  starting transfers between devices  109 us (21%)
  Pallas kernels  58.7 us (11%)
  local copies, waits for them, and re-layouts  14.6 us (3%)
  other arithmetic  13.4 us (3%)
    ppermute x12, waiting for transfers between devices, gather_parts(): near[step] = lax.ppermute(shard, 'fs', pairs)  170 us
    ppermute x16, waiting for transfers between devices, gather_parts(): far[step] = lax.ppermute(near[step], 'fs', swap)  141 us
    ppermute x12, starting transfers between devices, gather_parts(): near[step] = lax.ppermute(shard, 'fs', pairs)  76 us
    pallas_call x5, Pallas kernels, outward(): pl.pallas_call(functools.partial(outward_kernel, len(mine)), grid=(length...  24.1 us
    ppermute x16, starting transfers between devices, gather_parts(): far[step] = lax.ppermute(near[step], 'fs', swap)  21.5 us
    ppermute x5, waiting for transfers between devices, add_groups(): came = lax.ppermute(away, 'tp', [(0, 1), (1, 0)])  19.2 us
    pallas_call x1, Pallas kernels, recurrence(): pl.pallas_call(functools.partial(recurrence_kernel, len(mine)), grid=(blo...  17.8 us
    pallas_call x1, Pallas kernels, hidden_units(): pl.pallas_call(functools.partial(hidden_kernel, len(mine)), grid=(units /...  16.8 us
  transfers between devices with their start and end apart: 66, of which 24 were waited for; matrix products, arithmetic and copies ran while one was open for 3% of the time, Pallas kernels for 10%

commit v1 on v0

--- a/solution.py
+++ b/solution.py
@@ -35,12 +35,13 @@
     swap = [(at, at ^ 1) for at in range(count)]
     near = {0: shard}
     for step in visit_order(outer):
+        held, hop = (shard, step) if min(step, outer - step) == 1 else (near[step - 1], 1)
         pairs = [
-            (at * 2 + side, ((at - step) % outer) * 2 + side)
+            (at * 2 + side, ((at - hop) % outer) * 2 + side)
             for at in range(outer)
             for side in range(2)
         ]
-        near[step] = lax.ppermute(shard, "fs", pairs)
+        near[step] = lax.ppermute(held, "fs", pairs)
     far = {}
     for step in range(outer):
         far[step] = lax.ppermute(near[step], "fs", swap)

time: 531 us -> 401 us (0.76)
  the two profiles are of different devices: /device:TPU:26 before, /device:TPU:0 now
where the time goes in v1:
time: 401 us
  waiting for transfers between devices  257 us (64%)
  starting transfers between devices  59.9 us (15%)
  Pallas kernels  58.8 us (15%)
  other arithmetic  13.4 us (3%)
  local copies, waits for them, and re-layouts  11.3 us (3%)
    ppermute x16, waiting for transfers between devices, gather_parts(): far[step] = lax.ppermute(near[step], 'fs', swap)  140 us
    ppermute x12, waiting for transfers between devices, gather_parts(): near[step] = lax.ppermute(held, 'fs', pairs)  90.5 us
    ppermute x12, starting transfers between devices, gather_parts(): near[step] = lax.ppermute(held, 'fs', pairs)  26.8 us
    pallas_call x5, Pallas kernels, outward(): pl.pallas_call(functools.partial(outward_kernel, len(mine)), grid=(length...  24.1 us
    ppermute x16, starting transfers between devices, gather_parts(): far[step] = lax.ppermute(near[step], 'fs', swap)  21.7 us
    ppermute x5, waiting for transfers between devices, add_groups(): came = lax.ppermute(away, 'tp', [(0, 1), (1, 0)])  18.3 us
    pallas_call x1, Pallas kernels, recurrence(): pl.pallas_call(functools.partial(recurrence_kernel, len(mine)), grid=(blo...  17.8 us
    pallas_call x1, Pallas kernels, hidden_units(): pl.pallas_call(functools.partial(hidden_kernel, len(mine)), grid=(units /...  16.8 us
  transfers between devices with their start and end apart: 66, of which 28 were waited for; matrix products, arithmetic and copies ran while one was open for 4% of the time, Pallas kernels for 13%

profile of v1, /device:TPU:0, one launch (start us, length us, event | category | flops | bytes accessed | tf_op | source)
XLA Modules:
  0.0 400.7 jit_solution(13033801953879042333)
XLA Ops:
  1.1 5.1 %collective-permute-start.15 = (bf16[512,256]{1,0:T(8,128)(2,1)S(1)}, bf16[512,256]{1,0:T(8,128)(2,1)S(1)}, u32[]{:S(2)}, u32[]{:S(2)}) collective-permute-start(bf16[512,256]{1,0:T(8,128)(2,1)S(1)} %slice_select_fusion.1.refs_0_), channel_id=1, source_target_pairs={{0,12},{2,14},{4,0},{6,2},{8,4},{10,6},{12,8},{14,10},{1,13},{3,15... | collective-permute-start | bytes 786440 | tf_op jit(solution)/shard_map/ppermute | solution.py:44
  8.9 3.9 collective-permute-start
  14.4 5.0 %collective-permute-done.17.refs_3_ = bf16[512,256]{1,0:T(8,128)(2,1)S(1)} collective-permute-done((bf16[512,256]{1,0:T(8,128)(2,1)S(1)}, bf16[512,256]{1,0:T(8,128)(2,1)S(1)}, u32[]{:S(2)}, u32[]{:S(2)}) %collective-permute-start.17) | collective-permute-done | bytes 262176 | tf_op jit(solution)/shard_map/ppermute | solution.py:44
  20.0 1.8 collective-permute-done.22.refs_8_
  21.8 2.8 collective-permute-start.16
  24.6 5.2 %collective-permute-done.refs_1_ = bf16[256,1024]{1,0:T(8,128)(2,1)S(1)} collective-permute-done((bf16[256,1024]{1,0:T(8,128)(2,1)S(1)}, bf16[256,1024]{1,0:T(8,128)(2,1)S(1)}, u32[]{:S(2)}, u32[]{:S(2)}) %collective-permute-start) | collective-permute-done | bytes 524320 | tf_op jit(solution)/shard_map/ppermute | solution.py:44
  31.3 10.7 %collective-permute-done.2.refs_3_ = bf16[256,1024]{1,0:T(8,128)(2,1)S(1)} collective-permute-done((bf16[256,1024]{1,0:T(8,128)(2,1)S(1)}, bf16[256,1024]{1,0:T(8,128)(2,1)S(1)}, u32[]{:S(2)}, u32[]{:S(2)}) %collective-permute-start.2) | collective-permute-done | bytes 524320 | tf_op jit(solution)/shard_map/ppermute | solution.py:44
  44.1 2.6 collective-permute-done.16.refs_2_
  46.7 1.6 collective-permute-start.20
  51.3 4.6 %collective-permute-done.20.refs_6_ = bf16[512,256]{1,0:T(8,128)(2,1)S(1)} collective-permute-done((bf16[512,256]{1,0:T(8,128)(2,1)S(1)}, bf16[512,256]{1,0:T(8,128)(2,1)S(1)}, u32[]{:S(2)}, u32[]{:S(2)}) %collective-permute-start.20) | collective-permute-done | bytes 262176 | tf_op jit(solution)/shard_map/ppermute | solution.py:47
  58.3 8.9 %collective-permute-done.4.refs_5_ = bf16[256,1024]{1,0:T(8,128)(2,1)} collective-permute-done((bf16[256,1024]{1,0:T(8,128)(2,1)S(1)}, bf16[256,1024]{1,0:T(8,128)(2,1)}, u32[]{:S(2)}, u32[]{:S(2)}) %collective-permute-start.4) | collective-permute-done | bytes 524320 | tf_op jit(solution)/shard_map/ppermute | solution.py:47
  67.3 11.2 %collective-permute-done.6.refs_7_ = bf16[256,1024]{1,0:T(8,128)(2,1)} collective-permute-done((bf16[256,1024]{1,0:T(8,128)(2,1)S(1)}, bf16[256,1024]{1,0:T(8,128)(2,1)}, u32[]{:S(2)}, u32[]{:S(2)}) %collective-permute-start.6) | collective-permute-done | bytes 524320 | tf_op jit(solution)/shard_map/ppermute | solution.py:47
  79.1 10.1 %collective-permute-done.5.refs_6_ = bf16[256,1024]{1,0:T(8,128)(2,1)} collective-permute-done((bf16[256,1024]{1,0:T(8,128)(2,1)S(1)}, bf16[256,1024]{1,0:T(8,128)(2,1)}, u32[]{:S(2)}, u32[]{:S(2)}) %collective-permute-start.5) | collective-permute-done | bytes 524320 | tf_op jit(solution)/shard_map/ppermute | solution.py:47
  92.2 17.8 %shard_map.136.left_ref = bf16[512,1024]{1,0:T(8,128)(2,1)} custom-call(s32[9]{0:T(128)} %stack.39.meta, bf16[512,2048]{1,0:T(8,128)(2,1)} %x_ref.1, bf16[4,1024]{1,0:T(4,128)(2,1)} %taps_ref.1, bf16[4,256,256]{2,1,0:T(8,128)(2,1)} %rate_ref.1, bf16[4,256,256]{2,1,0:T(8,128)(2,1)} %inlet_ref.1, f32[1,1024]{1,0:T(1,128)} %bitcast.10, f32[512,1024]{1,0:T(8,128)} %shift_ref.1, ...), custom_call_target="tpu_custom_call" | custom-call | flops 4294967296 | bytes 12582912 | tf_op jit(solution)/shard_map/pallas_call | solution.py:153
  110.8 6.0 %shard_map.137 = bf16[512,2048]{1,0:T(8,128)(2,1)} custom-call(s32[9]{0:T(128)} %stack.39.meta, bf16[512,1024]{1,0:T(8,128)(2,1)} %shard_map.136.left_ref, bf16[512,256]{1,0:T(8,128)(2,1)} %copy-done.18, bf16[512,256]{1,0:T(8,128)(2,1)} %copy-done.33, bf16[512,256]{1,0:T(8,128)(2,1)} %copy-done.37, bf16[512,256]{1,0:T(8,128)(2,1)} %copy-done.34, ...), custom_call_target="tpu_custom_call" | custom-call | flops 2147483648 | bytes 4194304 | tf_op jit(solution)/shard_map/pallas_call | solution.py:227
  116.9 2.4 constant_dynamic-slice_fusion.4
  122.0 4.3 %collective-permute-start.32 = (bf16[256,2560]{1,0:T(8,128)(2,1)}, bf16[256,2560]{1,0:T(8,128)(2,1)}, u32[]{:S(2)}, u32[]{:S(2)}) collective-permute-start(bf16[256,2560]{1,0:T(8,128)(2,1)} %broadcast_select_fusion.refs_0_), channel_id=1, source_target_pairs={{0,12},{2,14},{4,0},{6,2},{8,4},{10,6},{12,8},{14,10},{1,13},{3,15... | collective-permute-start | bytes 3932168 | tf_op jit(solution)/shard_map/ppermute | solution.py:44
  126.4 3.9 collective-permute-start.47
  130.2 14.5 %collective-permute-done.30 = bf16[256,2048]{1,0:T(8,128)(2,1)} collective-permute-done((bf16[256,2048]{1,0:T(8,128)(2,1)}, bf16[256,2048]{1,0:T(8,128)(2,1)}, u32[]{:S(2)}, u32[]{:S(2)}) %collective-permute-start.30) | collective-permute-done | bytes 1048608 | tf_op jit(solution)/shard_map/ppermute | solution.py:252
  146.3 1.6 convert_add_fusion
  148.2 49.7 %collective-permute-done.47.refs_1_ = bf16[1280,256]{1,0:T(8,128)(2,1)} collective-permute-done((bf16[1280,256]{1,0:T(8,128)(2,1)S(1)}, bf16[1280,256]{1,0:T(8,128)(2,1)}, u32[]{:S(2)}, u32[]{:S(2)}) %collective-permute-start.47) | collective-permute-done | bytes 655392 | tf_op jit(solution)/shard_map/ppermute | solution.py:44
  197.8 1.5 collective-permute-start.35
  199.4 12.2 %collective-permute-done.48.refs_2_ = bf16[1280,256]{1,0:T(8,128)(2,1)} collective-permute-done((bf16[1280,256]{1,0:T(8,128)(2,1)S(1)}, bf16[1280,256]{1,0:T(8,128)(2,1)}, u32[]{:S(2)}, u32[]{:S(2)}) %collective-permute-start.48) | collective-permute-done | bytes 655392 | tf_op jit(solution)/shard_map/ppermute | solution.py:44
  212.2 3.6 collective-permute-done.50.refs_4_
  215.8 1.5 collective-permute-start.55
  217.8 1.7 collective-permute-start.33
  219.6 10.2 %collective-permute-done.35.refs_4_ = bf16[256,2560]{1,0:T(8,128)(2,1)} collective-permute-done((bf16[256,2560]{1,0:T(8,128)(2,1)}, bf16[256,2560]{1,0:T(8,128)(2,1)}, u32[]{:S(2)}, u32[]{:S(2)}) %collective-permute-start.35) | collective-permute-done | bytes 1310752 | tf_op jit(solution)/shard_map/ppermute | solution.py:47
  229.8 1.5 collective-permute-start.36
  231.7 4.6 %collective-permute-start.60 = (bf16[1280,256]{1,0:T(8,128)(2,1)}, bf16[1280,256]{1,0:T(8,128)(2,1)S(1)}, u32[]{:S(2)}, u32[]{:S(2)}) collective-permute-start(bf16[1280,256]{1,0:T(8,128)(2,1)} %collective-permute-done.47.refs_1_), channel_id=1, source_target_pairs={{0,12},{2,14},{4,0},{6,2},{8,4},{10,6},{12,8},{14,10},{1,13},{3,15... | collective-permute-start | bytes 1966088 | tf_op jit(solution)/shard_map/ppermute | solution.py:44
  236.3 7.4 %collective-permute-done.55.refs_0_ = bf16[1280,256]{1,0:T(8,128)(2,1)S(1)} collective-permute-done((bf16[1280,256]{1,0:T(8,128)(2,1)}, bf16[1280,256]{1,0:T(8,128)(2,1)S(1)}, u32[]{:S(2)}, u32[]{:S(2)}) %collective-permute-start.55) | collective-permute-done | bytes 655392 | tf_op jit(solution)/shard_map/ppermute | solution.py:47
  243.7 14.0 %collective-permute-done.56.refs_1_ = bf16[1280,256]{1,0:T(8,128)(2,1)S(1)} collective-permute-done((bf16[1280,256]{1,0:T(8,128)(2,1)}, bf16[1280,256]{1,0:T(8,128)(2,1)S(1)}, u32[]{:S(2)}, u32[]{:S(2)}) %collective-permute-start.56) | collective-permute-done | bytes 655392 | tf_op jit(solution)/shard_map/ppermute | solution.py:47
  258.3 4.1 %collective-permute-done.60.refs_0_ = bf16[1280,256]{1,0:T(8,128)(2,1)S(1)} collective-permute-done((bf16[1280,256]{1,0:T(8,128)(2,1)}, bf16[1280,256]{1,0:T(8,128)(2,1)S(1)}, u32[]{:S(2)}, u32[]{:S(2)}) %collective-permute-start.60) | collective-permute-done | bytes 655392 | tf_op jit(solution)/shard_map/ppermute | solution.py:44
  262.4 1.6 collective-permute-start.38
  265.3 20.6 %collective-permute-done.36.refs_5_ = bf16[256,2560]{1,0:T(8,128)(2,1)} collective-permute-done((bf16[256,2560]{1,0:T(8,128)(2,1)}, bf16[256,2560]{1,0:T(8,128)(2,1)}, u32[]{:S(2)}, u32[]{:S(2)}) %collective-permute-start.36) | collective-permute-done | bytes 1310752 | tf_op jit(solution)/shard_map/ppermute | solution.py:47
  286.5 27.6 %collective-permute-done.38.refs_7_ = bf16[256,2560]{1,0:T(8,128)(2,1)} collective-permute-done((bf16[256,2560]{1,0:T(8,128)(2,1)}, bf16[256,2560]{1,0:T(8,128)(2,1)}, u32[]{:S(2)}, u32[]{:S(2)}) %collective-permute-start.38) | collective-permute-done | bytes 1310752 | tf_op jit(solution)/shard_map/ppermute | solution.py:47
  314.7 24.4 %collective-permute-done.37.refs_6_ = bf16[256,2560]{1,0:T(8,128)(2,1)} collective-permute-done((bf16[256,2560]{1,0:T(8,128)(2,1)}, bf16[256,2560]{1,0:T(8,128)(2,1)}, u32[]{:S(2)}, u32[]{:S(2)}) %collective-permute-start.37) | collective-permute-done | bytes 1310752 | tf_op jit(solution)/shard_map/ppermute | solution.py:47
  339.8 1.6 pad_maximum_fusion.x_ref
  342.6 1.7 collective-permute-done.45.refs_14_
  344.4 1.6 collective-permute-start.63
  345.9 16.8 %shard_map.138.left_ref = bf16[512,2560]{1,0:T(8,128)(2,1)} custom-call(s32[9]{0:T(128)} %stack.39.meta, bf16[512,2048]{1,0:T(8,128)(2,1)} %pad_maximum_fusion.x_ref, bf16[256,2560]{1,0:T(8,128)(2,1)} %broadcast_select_fusion.refs_0_, bf16[256,2560]{1,0:T(8,128)(2,1)} %collective-permute-done.32.refs_1_, bf16[256,2560]{1,0:T(8,128)(2,1)} %collective-permute-done.33.refs_2_, ...), custom_call_target="tpu_custom_call" | custom-call | flops 10737418240 | bytes 20971520 | tf_op jit(solution)/shard_map/pallas_call | solution.py:191
  362.8 4.6 %shard_map.140 = bf16[512,512]{1,0:T(8,128)(2,1)} custom-call(s32[9]{0:T(128)} %stack.39.meta, bf16[512,2560]{1,0:T(8,128)(2,1)} %shard_map.138.left_ref, bf16[1280,256]{1,0:T(8,128)(2,1)} %copy-done.10, bf16[1280,256]{1,0:T(8,128)(2,1)} %copy-done.11, bf16[1280,256]{1,0:T(8,128)(2,1)} %copy-done.12, bf16[1280,256]{1,0:T(8,128)(2,1)} %copy-done.13), custom_call_target="tpu_custom_call" | custom-call | flops 1342177280 | bytes 2621440 | tf_op jit(solution)/shard_map/pallas_call | solution.py:227
  367.4 1.8 constant_dynamic-slice_fusion.2
  369.8 6.8 %shard_map.139 = bf16[512,1024]{1,0:T(8,128)(2,1)} custom-call(s32[9]{0:T(128)} %stack.39.meta, bf16[512,2560]{1,0:T(8,128)(2,1)} %shard_map.138.left_ref, bf16[1280,256]{1,0:T(8,128)(2,1)} %copy-done.16, bf16[1280,256]{1,0:T(8,128)(2,1)} %collective-permute-done.47.refs_1_, bf16[1280,256]{1,0:T(8,128)(2,1)} %collective-permute-done.48.refs_2_, ...), custom_call_target="tpu_custom_call" | custom-call | flops 2684354560 | bytes 5242880 | tf_op jit(solution)/shard_map/pallas_call | solution.py:227
  376.5 1.9 constant_dynamic-slice_fusion.3
  380.8 3.4 shard_map.141
  385.7 3.4 shard_map.142
  390.0 1.6 collective-permute-start.65
  396.3 1.9 collective-permute-done.65
  (225 shorter events, 42.6 us)
Async XLA Ops:
  8.9 21.0 %collective-permute-start = (bf16[256,1024]{1,0:T(8,128)(2,1)S(1)}, bf16[256,1024]{1,0:T(8,128)(2,1)S(1)}, u32[]{:S(2)}, u32[]{:S(2)}) collective-permute-start(bf16[256,1024]{1,0:T(8,128)(2,1)S(1)} %broadcast_select_fusion.3.refs_0_), channel_id=1, source_target_pairs={{0,12},{2,14},{4,0},{6,2},{8,4},{10,6},{12,8},{14,10},{1,13},{3,15... | collective-permute-start | bytes 1572872 | tf_op jit(solution)/shard_map/ppermute | solution.py:44
  12.7 29.3 %collective-permute-start.2 = (bf16[256,1024]{1,0:T(8,128)(2,1)S(1)}, bf16[256,1024]{1,0:T(8,128)(2,1)S(1)}, u32[]{:S(2)}, u32[]{:S(2)}) collective-permute-start(bf16[256,1024]{1,0:T(8,128)(2,1)S(1)} %broadcast_select_fusion.3.refs_0_), channel_id=1, source_target_pairs={{0,4},{2,6},{4,8},{6,10},{8,12},{10,14},{12,0},{14,2},{1,5},{3,7},... | collective-permute-start | bytes 1572872 | tf_op jit(solution)/shard_map/ppermute | solution.py:44
  12.9 29.6 %collective-permute-start.3 = (bf16[256,1024]{1,0:T(8,128)(2,1)S(1)}, bf16[256,1024]{1,0:T(8,128)(2,1)S(1)}, u32[]{:S(2)}, u32[]{:S(2)}) collective-permute-start(bf16[256,1024]{1,0:T(8,128)(2,1)S(1)} %broadcast_select_fusion.3.refs_0_), channel_id=1, source_target_pairs={{0,2},{2,0},{4,6},{6,4},{8,10},{10,8},{12,14},{14,12},{1,3},{3,1},... | collective-permute-start | bytes 1572872 | tf_op jit(solution)/shard_map/ppermute | solution.py:47
  19.5 24.6 %collective-permute-start.7 = (bf16[256,1024]{1,0:T(8,128)(2,1)S(1)}, bf16[256,1024]{1,0:T(8,128)(2,1)S(1)}, u32[]{:S(2)}, u32[]{:S(2)}) collective-permute-start(bf16[256,1024]{1,0:T(8,128)(2,1)S(1)} %broadcast_select_fusion.3.refs_0_), channel_id=1, source_target_pairs={{0,16},{16,0},{1,17},{17,1},{2,18},{18,2},{3,19},{19,3},{4,20},{20... | collective-permute-start | bytes 1572872 | tf_op jit(solution)/shard_map/ppermute | solution.py:51
  21.8 24.9 %collective-permute-start.16 = (bf16[512,256]{1,0:T(8,128)(2,1)S(1)}, bf16[512,256]{1,0:T(8,128)(2,1)S(1)}, u32[]{:S(2)}, u32[]{:S(2)}) collective-permute-start(bf16[512,256]{1,0:T(8,128)(2,1)S(1)} %collective-permute-done.15.refs_1_), channel_id=1, source_target_pairs={{0,12},{2,14},{4,0},{6,2},{8,4},{10,6},{12,8},{14,10},{1,13},{3,15... | collective-permute-start | bytes 786440 | tf_op jit(solution)/shard_map/ppermute | solution.py:44
  29.8 16.9 %collective-permute-start.19 = (bf16[512,256]{1,0:T(8,128)(2,1)S(1)}, bf16[512,256]{1,0:T(8,128)(2,1)S(1)}, u32[]{:S(2)}, u32[]{:S(2)}) collective-permute-start(bf16[512,256]{1,0:T(8,128)(2,1)S(1)} %collective-permute-done.15.refs_1_), channel_id=1, source_target_pairs={{0,2},{2,0},{4,6},{6,4},{8,10},{10,8},{12,14},{14,12},{1,3},{3,1},... | collective-permute-start | bytes 786440 | tf_op jit(solution)/shard_map/ppermute | solution.py:47
  42.0 14.8 %collective-permute-start.1 = (bf16[256,1024]{1,0:T(8,128)(2,1)S(1)}, bf16[256,1024]{1,0:T(8,128)(2,1)S(1)}, u32[]{:S(2)}, u32[]{:S(2)}) collective-permute-start(bf16[256,1024]{1,0:T(8,128)(2,1)S(1)} %collective-permute-done.refs_1_), channel_id=1, source_target_pairs={{0,12},{2,14},{4,0},{6,2},{8,4},{10,6},{12,8},{14,10},{1,13},{3,15... | collective-permute-start | bytes 1572872 | tf_op jit(solution)/shard_map/ppermute | solution.py:44
  49.2 18.1 %collective-permute-start.4 = (bf16[256,1024]{1,0:T(8,128)(2,1)S(1)}, bf16[256,1024]{1,0:T(8,128)(2,1)}, u32[]{:S(2)}, u32[]{:S(2)}) collective-permute-start(bf16[256,1024]{1,0:T(8,128)(2,1)S(1)} %collective-permute-done.refs_1_), channel_id=1, source_target_pairs={{0,2},{2,0},{4,6},{6,4},{8,10},{10,8},{12,14},{14,12},{1,3},{3,1},... | collective-permute-start | bytes 1572872 | tf_op jit(solution)/shard_map/ppermute | solution.py:47
  50.7 27.8 %collective-permute-start.6 = (bf16[256,1024]{1,0:T(8,128)(2,1)S(1)}, bf16[256,1024]{1,0:T(8,128)(2,1)}, u32[]{:S(2)}, u32[]{:S(2)}) collective-permute-start(bf16[256,1024]{1,0:T(8,128)(2,1)S(1)} %collective-permute-done.2.refs_3_), channel_id=1, source_target_pairs={{0,2},{2,0},{4,6},{6,4},{8,10},{10,8},{12,14},{14,12},{1,3},{3,1},... | collective-permute-start | bytes 1572872 | tf_op jit(solution)/shard_map/ppermute | solution.py:47
  51.2 27.3 %collective-permute-start.8 = (bf16[256,1024]{1,0:T(8,128)(2,1)S(1)}, bf16[256,1024]{1,0:T(8,128)(2,1)S(1)}, u32[]{:S(2)}, u32[]{:S(2)}) collective-permute-start(bf16[256,1024]{1,0:T(8,128)(2,1)S(1)} %collective-permute-done.refs_1_), channel_id=1, source_target_pairs={{0,16},{16,0},{1,17},{17,1},{2,18},{18,2},{3,19},{19,3},{4,20},{20... | collective-permute-start | bytes 1572872 | tf_op jit(solution)/shard_map/ppermute | solution.py:51
  55.9 23.1 %collective-permute-start.10 = (bf16[256,1024]{1,0:T(8,128)(2,1)S(1)}, bf16[256,1024]{1,0:T(8,128)(2,1)S(1)}, u32[]{:S(2)}, u32[]{:S(2)}) collective-permute-start(bf16[256,1024]{1,0:T(8,128)(2,1)S(1)} %collective-permute-done.2.refs_3_), channel_id=1, source_target_pairs={{0,16},{16,0},{1,17},{17,1},{2,18},{18,2},{3,19},{19,3},{4,20},{20... | collective-permute-start | bytes 1572872 | tf_op jit(solution)/shard_map/ppermute | solution.py:51
  56.8 32.4 %collective-permute-start.5 = (bf16[256,1024]{1,0:T(8,128)(2,1)S(1)}, bf16[256,1024]{1,0:T(8,128)(2,1)}, u32[]{:S(2)}, u32[]{:S(2)}) collective-permute-start(bf16[256,1024]{1,0:T(8,128)(2,1)S(1)} %collective-permute-done.1.refs_2_), channel_id=1, source_target_pairs={{0,2},{2,0},{4,6},{6,4},{8,10},{10,8},{12,14},{14,12},{1,3},{3,1},... | collective-permute-start | bytes 1572872 | tf_op jit(solution)/shard_map/ppermute | solution.py:47
  67.3 23.4 %collective-permute-start.11 = (bf16[256,1024]{1,0:T(8,128)(2,1)S(1)}, bf16[256,1024]{1,0:T(8,128)(2,1)}, u32[]{:S(2)}, u32[]{:S(2)}) collective-permute-start(bf16[256,1024]{1,0:T(8,128)(2,1)S(1)} %collective-permute-done.3.refs_4_), channel_id=1, source_target_pairs={{0,16},{16,0},{1,17},{17,1},{2,18},{18,2},{3,19},{19,3},{4,20},{20... | collective-permute-start | bytes 1572872 | tf_op jit(solution)/shard_map/ppermute | solution.py:51
  90.7 19.3 %collective-permute-start.26 = (bf16[512,256]{1,0:T(8,128)(2,1)}, bf16[512,256]{1,0:T(8,128)(2,1)S(1)}, u32[]{:S(2)}, u32[]{:S(2)}) collective-permute-start(bf16[512,256]{1,0:T(8,128)(2,1)} %copy-done.35), channel_id=1, source_target_pairs={{0,16},{16,0},{1,17},{17,1},{2,18},{18,2},{3,19},{19,3},{4,20},{20... | collective-permute-start | bytes 786440 | tf_op jit(solution)/shard_map/ppermute | solution.py:51
  91.1 18.9 %collective-permute-start.24 = (bf16[512,256]{1,0:T(8,128)(2,1)}, bf16[512,256]{1,0:T(8,128)(2,1)S(1)}, u32[]{:S(2)}, u32[]{:S(2)}) collective-permute-start(bf16[512,256]{1,0:T(8,128)(2,1)} %copy-done.37), channel_id=1, source_target_pairs={{0,16},{16,0},{1,17},{17,1},{2,18},{18,2},{3,19},{19,3},{4,20},{20... | collective-permute-start | bytes 786440 | tf_op jit(solution)/shard_map/ppermute | solution.py:51
  91.2 18.8 %collective-permute-start.27 = (bf16[512,256]{1,0:T(8,128)(2,1)}, bf16[512,256]{1,0:T(8,128)(2,1)}, u32[]{:S(2)}, u32[]{:S(2)}) collective-permute-start(bf16[512,256]{1,0:T(8,128)(2,1)} %copy-done.38), channel_id=1, source_target_pairs={{0,16},{16,0},{1,17},{17,1},{2,18},{18,2},{3,19},{19,3},{4,20},{20... | collective-permute-start | bytes 786440 | tf_op jit(solution)/shard_map/ppermute | solution.py:51
  91.6 18.4 %collective-permute-start.29 = (bf16[512,256]{1,0:T(8,128)(2,1)}, bf16[512,256]{1,0:T(8,128)(2,1)}, u32[]{:S(2)}, u32[]{:S(2)}) collective-permute-start(bf16[512,256]{1,0:T(8,128)(2,1)} %copy-done.39), channel_id=1, source_target_pairs={{0,16},{16,0},{1,17},{17,1},{2,18},{18,2},{3,19},{19,3},{4,20},{20... | collective-permute-start | bytes 786440 | tf_op jit(solution)/shard_map/ppermute | solution.py:51
  91.7 18.3 %collective-permute-start.28 = (bf16[512,256]{1,0:T(8,128)(2,1)}, bf16[512,256]{1,0:T(8,128)(2,1)}, u32[]{:S(2)}, u32[]{:S(2)}) collective-permute-start(bf16[512,256]{1,0:T(8,128)(2,1)} %copy-done.42), channel_id=1, source_target_pairs={{0,16},{16,0},{1,17},{17,1},{2,18},{18,2},{3,19},{19,3},{4,20},{20... | collective-permute-start | bytes 786440 | tf_op jit(solution)/shard_map/ppermute | solution.py:51
  119.3 25.5 %collective-permute-start.30 = (bf16[256,2048]{1,0:T(8,128)(2,1)}, bf16[256,2048]{1,0:T(8,128)(2,1)}, u32[]{:S(2)}, u32[]{:S(2)}) collective-permute-start(bf16[256,2048]{1,0:T(8,128)(2,1)} %constant_dynamic-slice_fusion.4), channel_id=1, source_target_pairs={{0,1},{1,0},{2,3},{3,2},{4,5},{5,4},{6,7},{7,6},{8,9},{9,8},{10,11... | collective-permute-start | bytes 3145736 | tf_op jit(solution)/shard_map/ppermute | solution.py:252
  122.0 95.3 %collective-permute-start.32 = (bf16[256,2560]{1,0:T(8,128)(2,1)}, bf16[256,2560]{1,0:T(8,128)(2,1)}, u32[]{:S(2)}, u32[]{:S(2)}) collective-permute-start(bf16[256,2560]{1,0:T(8,128)(2,1)} %broadcast_select_fusion.refs_0_), channel_id=1, source_target_pairs={{0,12},{2,14},{4,0},{6,2},{8,4},{10,6},{12,8},{14,10},{1,13},{3,15... | collective-permute-start | bytes 3932168 | tf_op jit(solution)/shard_map/ppermute | solution.py:44
  126.3 91.5 %collective-permute-start.34 = (bf16[256,2560]{1,0:T(8,128)(2,1)}, bf16[256,2560]{1,0:T(8,128)(2,1)}, u32[]{:S(2)}, u32[]{:S(2)}) collective-permute-start(bf16[256,2560]{1,0:T(8,128)(2,1)} %broadcast_select_fusion.refs_0_), channel_id=1, source_target_pairs={{0,4},{2,6},{4,8},{6,10},{8,12},{10,14},{12,0},{14,2},{1,5},{3,7},... | collective-permute-start | bytes 3932168 | tf_op jit(solution)/shard_map/ppermute | solution.py:44
  126.4 71.5 %collective-permute-start.47 = (bf16[1280,256]{1,0:T(8,128)(2,1)S(1)}, bf16[1280,256]{1,0:T(8,128)(2,1)}, u32[]{:S(2)}, u32[]{:S(2)}) collective-permute-start(bf16[1280,256]{1,0:T(8,128)(2,1)S(1)} %slice_select_fusion.refs_0_), channel_id=1, source_target_pairs={{0,12},{2,14},{4,0},{6,2},{8,4},{10,6},{12,8},{14,10},{1,13},{3,15... | collective-permute-start | bytes 1966088 | tf_op jit(solution)/shard_map/ppermute | solution.py:44
  130.2 81.3 %collective-permute-start.48 = (bf16[1280,256]{1,0:T(8,128)(2,1)S(1)}, bf16[1280,256]{1,0:T(8,128)(2,1)}, u32[]{:S(2)}, u32[]{:S(2)}) collective-permute-start(bf16[1280,256]{1,0:T(8,128)(2,1)S(1)} %slice_select_fusion.refs_0_), channel_id=1, source_target_pairs={{0,4},{2,6},{4,8},{6,10},{8,12},{10,14},{12,0},{14,2},{1,5},{3,7},... | collective-permute-start | bytes 1966088 | tf_op jit(solution)/shard_map/ppermute | solution.py:44
  144.8 66.8 %collective-permute-start.49 = (bf16[1280,256]{1,0:T(8,128)(2,1)S(1)}, bf16[1280,256]{1,0:T(8,128)(2,1)}, u32[]{:S(2)}, u32[]{:S(2)}) collective-permute-start(bf16[1280,256]{1,0:T(8,128)(2,1)S(1)} %slice_select_fusion.refs_0_), channel_id=1, source_target_pairs={{0,2},{2,0},{4,6},{6,4},{8,10},{10,8},{12,14},{14,12},{1,3},{3,1},... | collective-permute-start | bytes 1966088 | tf_op jit(solution)/shard_map/ppermute | solution.py:47
  197.8 32.0 %collective-permute-start.35 = (bf16[256,2560]{1,0:T(8,128)(2,1)}, bf16[256,2560]{1,0:T(8,128)(2,1)}, u32[]{:S(2)}, u32[]{:S(2)}) collective-permute-start(bf16[256,2560]{1,0:T(8,128)(2,1)} %broadcast_select_fusion.refs_0_), channel_id=1, source_target_pairs={{0,2},{2,0},{4,6},{6,4},{8,10},{10,8},{12,14},{14,12},{1,3},{3,1},... | collective-permute-start | bytes 3932168 | tf_op jit(solution)/shard_map/ppermute | solution.py:47
  211.6 20.1 %collective-permute-start.39 = (bf16[256,2560]{1,0:T(8,128)(2,1)}, bf16[256,2560]{1,0:T(8,128)(2,1)S(1)}, u32[]{:S(2)}, u32[]{:S(2)}) collective-permute-start(bf16[256,2560]{1,0:T(8,128)(2,1)} %broadcast_select_fusion.refs_0_), channel_id=1, source_target_pairs={{0,16},{16,0},{1,17},{17,1},{2,18},{18,2},{3,19},{19,3},{4,20},{20... | collective-permute-start | bytes 3932168 | tf_op jit(solution)/shard_map/ppermute | solution.py:51
  215.8 28.0 %collective-permute-start.55 = (bf16[1280,256]{1,0:T(8,128)(2,1)}, bf16[1280,256]{1,0:T(8,128)(2,1)S(1)}, u32[]{:S(2)}, u32[]{:S(2)}) collective-permute-start(bf16[1280,256]{1,0:T(8,128)(2,1)} %collective-permute-done.47.refs_1_), channel_id=1, source_target_pairs={{0,2},{2,0},{4,6},{6,4},{8,10},{10,8},{12,14},{14,12},{1,3},{3,1},... | collective-permute-start | bytes 1966088 | tf_op jit(solution)/shard_map/ppermute | solution.py:47
  217.3 40.5 %collective-permute-start.56 = (bf16[1280,256]{1,0:T(8,128)(2,1)}, bf16[1280,256]{1,0:T(8,128)(2,1)S(1)}, u32[]{:S(2)}, u32[]{:S(2)}) collective-permute-start(bf16[1280,256]{1,0:T(8,128)(2,1)} %collective-permute-done.48.refs_2_), channel_id=1, source_target_pairs={{0,2},{2,0},{4,6},{6,4},{8,10},{10,8},{12,14},{14,12},{1,3},{3,1},... | collective-permute-start | bytes 1966088 | tf_op jit(solution)/shard_map/ppermute | solution.py:47
  217.8 46.4 %collective-permute-start.33 = (bf16[256,2560]{1,0:T(8,128)(2,1)}, bf16[256,2560]{1,0:T(8,128)(2,1)}, u32[]{:S(2)}, u32[]{:S(2)}) collective-permute-start(bf16[256,2560]{1,0:T(8,128)(2,1)} %collective-permute-done.32.refs_1_), channel_id=1, source_target_pairs={{0,12},{2,14},{4,0},{6,2},{8,4},{10,6},{12,8},{14,10},{1,13},{3,15... | collective-permute-start | bytes 3932168 | tf_op jit(solution)/shard_map/ppermute | solution.py:44
  229.8 56.2 %collective-permute-start.36 = (bf16[256,2560]{1,0:T(8,128)(2,1)}, bf16[256,2560]{1,0:T(8,128)(2,1)}, u32[]{:S(2)}, u32[]{:S(2)}) collective-permute-start(bf16[256,2560]{1,0:T(8,128)(2,1)} %collective-permute-done.32.refs_1_), channel_id=1, source_target_pairs={{0,2},{2,0},{4,6},{6,4},{8,10},{10,8},{12,14},{14,12},{1,3},{3,1},... | collective-permute-start | bytes 3932168 | tf_op jit(solution)/shard_map/ppermute | solution.py:47
  231.7 30.6 %collective-permute-start.60 = (bf16[1280,256]{1,0:T(8,128)(2,1)}, bf16[1280,256]{1,0:T(8,128)(2,1)S(1)}, u32[]{:S(2)}, u32[]{:S(2)}) collective-permute-start(bf16[1280,256]{1,0:T(8,128)(2,1)} %collective-permute-done.47.refs_1_), channel_id=1, source_target_pairs={{0,12},{2,14},{4,0},{6,2},{8,4},{10,6},{12,8},{14,10},{1,13},{3,15... | collective-permute-start | bytes 1966088 | tf_op jit(solution)/shard_map/ppermute | solution.py:44
  243.7 18.6 %collective-permute-start.57 = (bf16[1280,256]{1,0:T(8,128)(2,1)S(1)}, bf16[1280,256]{1,0:T(8,128)(2,1)S(1)}, u32[]{:S(2)}, u32[]{:S(2)}) collective-permute-start(bf16[1280,256]{1,0:T(8,128)(2,1)S(1)} %collective-permute-done.55.refs_0_), channel_id=1, source_target_pairs={{0,16},{16,0},{1,17},{17,1},{2,18},{18,2},{3,19},{19,3},{4,20},{20... | collective-permute-start | bytes 1966088 | tf_op jit(solution)/shard_map/ppermute | solution.py:51
  262.4 51.7 %collective-permute-start.40 = (bf16[256,2560]{1,0:T(8,128)(2,1)}, bf16[256,2560]{1,0:T(8,128)(2,1)S(1)}, u32[]{:S(2)}, u32[]{:S(2)}) collective-permute-start(bf16[256,2560]{1,0:T(8,128)(2,1)} %collective-permute-done.32.refs_1_), channel_id=1, source_target_pairs={{0,16},{16,0},{1,17},{17,1},{2,18},{18,2},{3,19},{19,3},{4,20},{20... | collective-permute-start | bytes 3932168 | tf_op jit(solution)/shard_map/ppermute | solution.py:51
  262.4 51.7 %collective-permute-start.38 = (bf16[256,2560]{1,0:T(8,128)(2,1)}, bf16[256,2560]{1,0:T(8,128)(2,1)}, u32[]{:S(2)}, u32[]{:S(2)}) collective-permute-start(bf16[256,2560]{1,0:T(8,128)(2,1)} %collective-permute-done.34.refs_3_), channel_id=1, source_target_pairs={{0,2},{2,0},{4,6},{6,4},{8,10},{10,8},{12,14},{14,12},{1,3},{3,1},... | collective-permute-start | bytes 3932168 | tf_op jit(solution)/shard_map/ppermute | solution.py:47
  264.0 50.6 %collective-permute-start.42 = (bf16[256,2560]{1,0:T(8,128)(2,1)}, bf16[256,2560]{1,0:T(8,128)(2,1)S(1)}, u32[]{:S(2)}, u32[]{:S(2)}) collective-permute-start(bf16[256,2560]{1,0:T(8,128)(2,1)} %collective-permute-done.34.refs_3_), channel_id=1, source_target_pairs={{0,16},{16,0},{1,17},{17,1},{2,18},{18,2},{3,19},{19,3},{4,20},{20... | collective-permute-start | bytes 3932168 | tf_op jit(solution)/shard_map/ppermute | solution.py:51
  264.2 74.9 %collective-permute-start.37 = (bf16[256,2560]{1,0:T(8,128)(2,1)}, bf16[256,2560]{1,0:T(8,128)(2,1)}, u32[]{:S(2)}, u32[]{:S(2)}) collective-permute-start(bf16[256,2560]{1,0:T(8,128)(2,1)} %collective-permute-done.33.refs_2_), channel_id=1, source_target_pairs={{0,2},{2,0},{4,6},{6,4},{8,10},{10,8},{12,14},{14,12},{1,3},{3,1},... | collective-permute-start | bytes 3932168 | tf_op jit(solution)/shard_map/ppermute | solution.py:47
  286.0 53.1 %collective-permute-start.31 = (bf16[256,2048]{1,0:T(8,128)(2,1)S(1)}, bf16[256,2048]{1,0:T(8,128)(2,1)S(1)}, u32[]{:S(2)}, u32[]{:S(2)}) collective-permute-start(bf16[256,2048]{1,0:T(8,128)(2,1)S(1)} %multiply_convert_fusion.1), channel_id=1, source_target_pairs={{0,1},{1,0},{2,3},{3,2},{4,5},{5,4},{6,7},{7,6},{8,9},{9,8},{10,11... | collective-permute-start | bytes 3145736 | tf_op jit(solution)/shard_map/ppermute | solution.py:281
  314.1 27.4 %collective-permute-start.43 = (bf16[256,2560]{1,0:T(8,128)(2,1)}, bf16[256,2560]{1,0:T(8,128)(2,1)}, u32[]{:S(2)}, u32[]{:S(2)}) collective-permute-start(bf16[256,2560]{1,0:T(8,128)(2,1)} %collective-permute-done.35.refs_4_), channel_id=1, source_target_pairs={{0,16},{16,0},{1,17},{17,1},{2,18},{18,2},{3,19},{19,3},{4,20},{20... | collective-permute-start | bytes 3932168 | tf_op jit(solution)/shard_map/ppermute | solution.py:51
  314.1 27.4 %collective-permute-start.41 = (bf16[256,2560]{1,0:T(8,128)(2,1)}, bf16[256,2560]{1,0:T(8,128)(2,1)}, u32[]{:S(2)}, u32[]{:S(2)}) collective-permute-start(bf16[256,2560]{1,0:T(8,128)(2,1)} %collective-permute-done.33.refs_2_), channel_id=1, source_target_pairs={{0,16},{16,0},{1,17},{17,1},{2,18},{18,2},{3,19},{19,3},{4,20},{20... | collective-permute-start | bytes 3932168 | tf_op jit(solution)/shard_map/ppermute | solution.py:51
  314.6 27.4 %collective-permute-start.44 = (bf16[256,2560]{1,0:T(8,128)(2,1)}, bf16[256,2560]{1,0:T(8,128)(2,1)}, u32[]{:S(2)}, u32[]{:S(2)}) collective-permute-start(bf16[256,2560]{1,0:T(8,128)(2,1)} %collective-permute-done.36.refs_5_), channel_id=1, source_target_pairs={{0,16},{16,0},{1,17},{17,1},{2,18},{18,2},{3,19},{19,3},{4,20},{20... | collective-permute-start | bytes 3932168 | tf_op jit(solution)/shard_map/ppermute | solution.py:51
  341.4 27.8 %collective-permute-start.51 = (bf16[1280,256]{1,0:T(8,128)(2,1)}, bf16[1280,256]{1,0:T(8,128)(2,1)}, u32[]{:S(2)}, u32[]{:S(2)}) collective-permute-start(bf16[1280,256]{1,0:T(8,128)(2,1)} %collective-permute-done.47.refs_1_), channel_id=1, source_target_pairs={{0,16},{16,0},{1,17},{17,1},{2,18},{18,2},{3,19},{19,3},{4,20},{20... | collective-permute-start | bytes 1966088 | tf_op jit(solution)/shard_map/ppermute | solution.py:51
  341.4 28.3 %collective-permute-start.52 = (bf16[1280,256]{1,0:T(8,128)(2,1)}, bf16[1280,256]{1,0:T(8,128)(2,1)}, u32[]{:S(2)}, u32[]{:S(2)}) collective-permute-start(bf16[1280,256]{1,0:T(8,128)(2,1)} %collective-permute-done.48.refs_2_), channel_id=1, source_target_pairs={{0,16},{16,0},{1,17},{17,1},{2,18},{18,2},{3,19},{19,3},{4,20},{20... | collective-permute-start | bytes 1966088 | tf_op jit(solution)/shard_map/ppermute | solution.py:51
  341.9 27.8 %collective-permute-start.53 = (bf16[1280,256]{1,0:T(8,128)(2,1)}, bf16[1280,256]{1,0:T(8,128)(2,1)}, u32[]{:S(2)}, u32[]{:S(2)}) collective-permute-start(bf16[1280,256]{1,0:T(8,128)(2,1)} %collective-permute-done.49.refs_3_), channel_id=1, source_target_pairs={{0,16},{16,0},{1,17},{17,1},{2,18},{18,2},{3,19},{19,3},{4,20},{20... | collective-permute-start | bytes 1966088 | tf_op jit(solution)/shard_map/ppermute | solution.py:51
  342.5 37.4 %collective-permute-start.61 = (bf16[1280,256]{1,0:T(8,128)(2,1)S(1)}, bf16[1280,256]{1,0:T(8,128)(2,1)S(1)}, u32[]{:S(2)}, u32[]{:S(2)}) collective-permute-start(bf16[1280,256]{1,0:T(8,128)(2,1)S(1)} %collective-permute-done.60.refs_0_), channel_id=1, source_target_pairs={{0,16},{16,0},{1,17},{17,1},{2,18},{18,2},{3,19},{19,3},{4,20},{20... | collective-permute-start | bytes 1966088 | tf_op jit(solution)/shard_map/ppermute | solution.py:51
  344.4 23.0 %collective-permute-start.63 = (bf16[1280,256]{1,0:T(8,128)(2,1)S(1)}, bf16[1280,256]{1,0:T(8,128)(2,1)S(1)}, u32[]{:S(2)}, u32[]{:S(2)}) collective-permute-start(bf16[1280,256]{1,0:T(8,128)(2,1)S(1)} %collective-permute-done.60.refs_0_), channel_id=1, source_target_pairs={{0,2},{2,0},{4,6},{6,4},{8,10},{10,8},{12,14},{14,12},{1,3},{3,1},... | collective-permute-start | bytes 1966088 | tf_op jit(solution)/shard_map/ppermute | solution.py:47
  367.3 18.4 %collective-permute-start.64 = (bf16[1280,256]{1,0:T(8,128)(2,1)S(1)}, bf16[1280,256]{1,0:T(8,128)(2,1)}, u32[]{:S(2)}, u32[]{:S(2)}) collective-permute-start(bf16[1280,256]{1,0:T(8,128)(2,1)S(1)} %collective-permute-done.63.refs_0_), channel_id=1, source_target_pairs={{0,16},{16,0},{1,17},{17,1},{2,18},{18,2},{3,19},{19,3},{4,20},{20... | collective-permute-start | bytes 1966088 | tf_op jit(solution)/shard_map/ppermute | solution.py:51
  369.2 22.3 %collective-permute-start.59 = (bf16[256,512]{1,0:T(8,128)(2,1)}, bf16[256,512]{1,0:T(8,128)(2,1)}, u32[]{:S(2)}, u32[]{:S(2)}) collective-permute-start(bf16[256,512]{1,0:T(8,128)(2,1)} %constant_dynamic-slice_fusion.2), channel_id=1, source_target_pairs={{0,1},{1,0},{2,3},{3,2},{4,5},{5,4},{6,7},{7,6},{8,9},{9,8},{10,11... | collective-permute-start | bytes 786440 | tf_op jit(solution)/shard_map/ppermute | solution.py:252
  378.4 15.1 %collective-permute-start.54 = (bf16[256,1024]{1,0:T(8,128)(2,1)}, bf16[256,1024]{1,0:T(8,128)(2,1)}, u32[]{:S(2)}, u32[]{:S(2)}) collective-permute-start(bf16[256,1024]{1,0:T(8,128)(2,1)} %constant_dynamic-slice_fusion.3), channel_id=1, source_target_pairs={{0,1},{1,0},{2,3},{3,2},{4,5},{5,4},{6,7},{7,6},{8,9},{9,8},{10,11... | collective-permute-start | bytes 1572872 | tf_op jit(solution)/shard_map/ppermute | solution.py:252
  (63 other events, 1552.8 us)
